TPU v7x, 128 devices: a whole 4x4x4 slice. The times are simulated.
128 devices in a mesh: sp: 16 (over z, y), tp: 8 (over x, core).
Axes of the slice: x: 4, y: 4, z: 4, core: 2. Of those that a mesh axis runs over, the one named last changes fastest.
Arguments:
- latent: bfloat16 [2048, 4096], P(('sp', 'tp')), may hold values from -8 to 8
- context: bfloat16 [512, 4096], P('sp'), may hold values from -6 to 6
- condition: float32 [4096], P('sp'), may hold values from -6 to 6
- context_condition: float32 [4096], P('sp'), may hold values from -6 to 6
- shift_weight: bfloat16 [4096, 4096], P('sp', 'tp'), may hold values from -0.09375 to 0.09375
- scale_weight: bfloat16 [4096, 4096], P('sp', 'tp'), may hold values from -0.09375 to 0.09375
- gate_weight: bfloat16 [4096, 4096], P('sp', 'tp'), may hold values from -0.09375 to 0.09375
- norm_gain: float32 [4096], replicated, may hold values from 0.1 to 1.9
- decay_down: bfloat16 [4096, 128], replicated, may hold values from -0.09375 to 0.09375
- decay_up: bfloat16 [128, 4096], P(None, 'tp'), may hold values from -0.5 to 0.5
- rate_down: bfloat16 [4096, 128], replicated, may hold values from -0.09375 to 0.09375
- rate_up: bfloat16 [128, 4096], P(None, 'tp'), may hold values from -0.5 to 0.5
- head_bias: float32 [2, 4096], P(None, 'tp'), may hold values from -12 to 1
- query_weight: bfloat16 [4096, 4096], P(None, 'tp'), may hold values from -0.09375 to 0.09375
- key_weight: bfloat16 [4096, 4096], P(None, 'tp'), may hold values from -0.09375 to 0.09375
- value_weight: bfloat16 [4096, 4096], P(None, 'tp'), may hold values from -0.09375 to 0.09375
- branch_weight: bfloat16 [4096, 4096], P(None, 'tp'), may hold values from -0.09375 to 0.09375
- group_gain: float32 [4096], P('tp'), may hold values from 0.1 to 1.9
- out_weight: bfloat16 [4096, 4096], P('tp'), may hold values from -0.09375 to 0.09375
Outputs:
- updated: bfloat16 [2048, 4096], P(('sp', 'tp'))
All inputs are finite; a program needn't handle non-finite values.
Results may differ from a plain program's by a relative error of at most 0.017.
Values may be sent and summed in bfloat16 or wider, within the bound.
A program may use at most 128 MiB of HBM per device.

v0:
```python
import math

import jax
import jax.numpy as jnp
from jax import lax
from jax.sharding import PartitionSpec as P

HEAD_DIM = 64


NORM_EPS = 1e-06
GROUP_EPS = 0.00064
DECAY_TOP = math.exp(-0.5)
block_rows = 64


def copy_for_each(value, axis):
    copies = jnp.broadcast_to(value, (lax.axis_size(axis), *value.shape))
    return lax.all_to_all(copies, axis, split_axis=0, concat_axis=0, tiled=True)


def over_copies(value, axis):
    return copy_for_each(value, axis).sum(axis=0)


def together(arrays, axis):
    vector, at, outs = (jnp.concatenate([a.reshape(-1) for a in arrays]), 0, [])
    total = over_copies(vector, axis)
    for a in arrays:
        outs.append(total[at : at + a.size].reshape(a.shape))
        at += a.size
    return tuple(outs)


def sent_together(arrays, axis, dim, along):
    both = jnp.concatenate(arrays, axis=along)
    filled, at, outs = (lax.all_gather(both, axis, axis=dim, tiled=True), 0, [])
    for a in arrays:
        outs.append(lax.slice_in_dim(filled, at, at + a.shape[along], axis=along))
        at += a.shape[along]
    return tuple(outs)


def joined_along(parts, dim):
    parts = jnp.moveaxis(parts, 0, dim)
    shape = parts.shape
    return parts.reshape(*shape[:dim], shape[dim] * shape[dim + 1], *shape[dim + 2 :])


def gathered_copies(value, axis, dim):
    return joined_along(copy_for_each(value, axis), dim)


def gather_packed(arrays, axis, dims):
    vector = jnp.concatenate([a.reshape(-1) for a in arrays])
    lines, at, outs = (lax.all_gather(vector, axis), 0, [])
    for a, dim in zip(arrays, dims):
        parts = lines[:, at : at + a.size].reshape(-1, *a.shape)
        outs.append(joined_along(parts, dim))
        at += a.size
    return tuple(outs)


def combined_pairwise(pieces, combine):
    while len(jax.tree.leaves(pieces)[0]) > 1:
        pieces = jax.vmap(combine)(
            *(jax.tree.map(lambda part: part[side::2], pieces) for side in (0, 1))
        )
    return jax.tree.map(lambda part: part[0], pieces)


def carried_in(value, axis, combine, identity, reverse):
    devices, position = (lax.axis_size(axis), lax.axis_index(axis))
    passed = jnp.arange(devices) > position if reverse else jnp.arange(devices) < position

    def kept(part, zero, own):
        part = jnp.where(
            passed.reshape(-1, *(1 for _ in own.shape)),
            part.astype(own.dtype),
            jnp.asarray(zero, own.dtype),
        )
        return part[::-1] if reverse else part

    pieces = jax.tree.map(
        lambda part: copy_for_each(part, axis),
        jax.tree.map(
            lambda part, kind: part.astype(kind),
            value,
            jax.tree.map(lambda a: jnp.bfloat16 if a.dtype == jnp.float32 else a.dtype, value),
        ),
    )
    return combined_pairwise(jax.tree.map(kept, pieces, identity, value), combine)


def in_blocks(value, dim, devices):
    before, after = (value.shape[:dim], value.shape[dim + 1 :])
    return jnp.moveaxis(value.reshape(*before, devices, -1, *after), dim, 0)


def summed_on_arrival(value, axis, dim):
    devices = lax.axis_size(axis)
    parts = lax.all_to_all(in_blocks(value, dim, devices), axis, 0, 0, tiled=True)
    return jnp.sum(parts.astype(jnp.float32), axis=0)


def product(form, left, right):
    return jnp.einsum(form, left, right)


def compose(earlier, later):
    return (
        product("...jk,...kl->...jl", earlier[0], later[0]),
        product("...ik,...kl->...il", earlier[1], later[0]) + later[1],
    )


def modulated(rows, gain, scale, shift):
    values = rows.astype(jnp.float32)
    inverse = lax.rsqrt(jnp.mean(values * values, axis=-1, keepdims=True) + NORM_EPS)
    return (values * inverse * gain * (1.0 + scale) + shift).astype(jnp.bfloat16)


def chain_inputs(keys, values, decay_pre, rate_pre, head_bias):
    rows = keys.shape[0]
    log_decay = -DECAY_TOP * jax.nn.sigmoid(head_bias[0] + decay_pre.astype(jnp.float32))
    rate = jax.nn.sigmoid(head_bias[1] + rate_pre.astype(jnp.float32))
    key_heads = keys.astype(jnp.float32).reshape(rows, -1, HEAD_DIM)
    unit = key_heads * lax.rsqrt(jnp.sum(key_heads * key_heads, axis=-1, keepdims=True) + 1.0)
    value_heads = values.astype(jnp.float32).reshape(rows, -1, HEAD_DIM)
    write = unit * rate.reshape(rows, -1, HEAD_DIM)
    return (key_heads, value_heads, -unit, write, log_decay.reshape(rows, -1, HEAD_DIM))


def to_blocks(array, length):
    rows, heads, width = array.shape
    return array.reshape(rows // length, length, heads, width).transpose(0, 2, 1, 3)


def block_terms(keys, values, erase, write, log_decay):
    length = keys.shape[2]
    width = keys.shape[3]
    row_index = lax.broadcasted_iota(jnp.int32, (length, length), 0)
    col_index = lax.broadcasted_iota(jnp.int32, (length, length), 1)
    inclusive = (row_index >= col_index).astype(jnp.float32)
    strict = (row_index > col_index).astype(jnp.float32)
    cumulative = product("ts,bhsn->bhtn", inclusive, log_decay)
    final = cumulative[:, :, -1:, :]
    erase_scaled = erase * jnp.exp(cumulative - log_decay)
    growth = jnp.exp(-cumulative)
    write_scaled = write * growth
    key_scaled = keys * growth
    coupling = product("bhtn,bhsn->bhts", erase_scaled, write_scaled) * strict
    feeding = product("bhtn,bhsn->bhts", erase_scaled, key_scaled) * strict
    right_side = jnp.concatenate(
        [erase_scaled, product("bhts,bhsn->bhtn", feeding, values)], axis=-1
    )
    system = jnp.eye(length, dtype=jnp.float32) - coupling
    solved = jax.scipy.linalg.solve_triangular(system, right_side, lower=True, unit_diagonal=True)
    response = solved[..., :width]
    offset = solved[..., width:]
    tail = jnp.exp(final - cumulative)
    write_tail = write * tail
    key_tail = keys * tail
    diagonal = jnp.exp(final[:, :, 0, :])
    transfer = product("bhtj,bhtl->bhjl", response, write_tail) + diagonal[..., :, None] * jnp.eye(
        width, dtype=jnp.float32
    )
    constant = product("bhti,bhtl->bhil", offset, write_tail) + product(
        "bhti,bhtl->bhil", values, key_tail
    )
    pieces = (cumulative, inclusive, response, offset, write_scaled, key_scaled)
    return (transfer, constant, pieces)


def context_map(inputs, flip):
    arrays = inputs
    if flip:
        arrays = tuple((jnp.flip(array, 0) for array in arrays))
    length = arrays[0].shape[0]
    keys, values, erase, write, log_decay = (to_blocks(array, length) for array in arrays)
    transfer, constant, pieces = block_terms(keys, values, erase, write, log_decay)
    return (transfer[0], constant[0])


def latent_blocks(query_heads, inputs, flip):
    arrays = (query_heads,) + inputs
    if flip:
        arrays = tuple((jnp.flip(array, 0) for array in arrays))
    length = min(block_rows, arrays[0].shape[0])
    queries, keys, values, erase, write, log_decay = (to_blocks(array, length) for array in arrays)
    transfer, constant, pieces = block_terms(keys, values, erase, write, log_decay)
    ahead = lax.associative_scan(compose, (transfer, constant), axis=0)
    heads, width = (transfer.shape[1], transfer.shape[2])
    unit = jnp.broadcast_to(jnp.eye(width, dtype=jnp.float32), (1, heads, width, width))
    before = (
        jnp.concatenate([unit, ahead[0][:-1]], axis=0),
        jnp.concatenate([jnp.zeros_like(unit), ahead[1][:-1]], axis=0),
    )
    return ((ahead[0][-1], ahead[1][-1]), before, queries, values, pieces)


def latent_read(start, blocks, flip):
    device_map, before, queries, values, pieces = blocks
    cumulative, inclusive, response, offset, write_scaled, key_scaled = pieces
    starts = product("hij,bhjk->bhik", start, before[0]) + before[1]
    query_scaled = queries * jnp.exp(cumulative)
    attend_write = product("bhtn,bhsn->bhts", query_scaled, write_scaled) * inclusive
    attend_key = product("bhtn,bhsn->bhts", query_scaled, key_scaled) * inclusive
    removed = product("bhtj,bhij->bhti", response, starts) + offset
    read = (
        product("bhtj,bhij->bhti", query_scaled, starts)
        + product("bhts,bhsi->bhti", attend_write, removed)
        + product("bhts,bhsi->bhti", attend_key, values)
    )
    count, heads, length, width = read.shape
    read = read.transpose(0, 2, 1, 3).reshape(count * length, heads, width)
    if flip:
        read = jnp.flip(read, 0)
    return read


def fold_state(state, pair):
    return (product("hij,hjk->hik", state, pair[0]) + pair[1], None)


def on_device(
    latent,
    context,
    condition,
    context_condition,
    shift_weight,
    scale_weight,
    gate_weight,
    norm_gain,
    decay_down,
    decay_up,
    rate_down,
    rate_up,
    head_bias,
    query_weight,
    key_weight,
    value_weight,
    branch_weight,
    group_gain,
    out_weight,
):
    local = query_weight.shape[1]
    conditions = jax.nn.silu(jnp.stack([condition, context_condition])).astype(jnp.bfloat16)
    shift_part = jnp.dot(conditions, shift_weight, preferred_element_type=jnp.float32)
    scale_part = jnp.dot(conditions, scale_weight, preferred_element_type=jnp.float32)
    gate_part = jnp.dot(conditions[:1], gate_weight, preferred_element_type=jnp.float32)
    summed = together((shift_part, scale_part, gate_part), "sp")
    shift, scale, gate = sent_together((summed[0], summed[1], summed[2]), "tp", 1, 0)
    normed = modulated(latent, norm_gain, scale[0], shift[0])
    decay_low = jnp.tanh(jnp.dot(normed, decay_down, preferred_element_type=jnp.float32)).astype(
        jnp.bfloat16
    )
    rate_low = jnp.dot(normed, rate_down, preferred_element_type=jnp.float32).astype(jnp.bfloat16)
    packed = jnp.concatenate([normed, decay_low, rate_low], axis=1)
    model_width = normed.shape[1]
    rank = decay_low.shape[1]
    piece = gathered_copies(packed, "tp", 0)
    rows_in = piece[:, :model_width]
    outputs = [
        jnp.dot(rows_in, weight, preferred_element_type=jnp.float32).astype(jnp.bfloat16)
        for weight in (query_weight, key_weight, value_weight, branch_weight)
    ]
    outputs.append(
        jnp.dot(
            piece[:, model_width : model_width + rank], decay_up, preferred_element_type=jnp.float32
        ).astype(jnp.bfloat16)
    )
    outputs.append(
        jnp.dot(piece[:, model_width + rank :], rate_up, preferred_element_type=jnp.float32).astype(
            jnp.bfloat16
        )
    )
    projected = jnp.concatenate(outputs, axis=1)
    queries = projected[:, :local]
    keys = projected[:, local : 2 * local]
    values = projected[:, 2 * local : 3 * local]
    branch = projected[:, 3 * local : 4 * local]
    decay_pre = projected[:, 4 * local : 5 * local]
    rate_pre = projected[:, 5 * local :]
    normed_context = modulated(context, norm_gain, scale[1], shift[1])
    context_keys = jnp.dot(normed_context, key_weight, preferred_element_type=jnp.float32).astype(
        jnp.bfloat16
    )
    context_values = jnp.dot(
        normed_context, value_weight, preferred_element_type=jnp.float32
    ).astype(jnp.bfloat16)
    context_decay_low = jnp.tanh(
        jnp.dot(normed_context, decay_down, preferred_element_type=jnp.float32)
    ).astype(jnp.bfloat16)
    context_rate_low = jnp.dot(
        normed_context, rate_down, preferred_element_type=jnp.float32
    ).astype(jnp.bfloat16)
    context_decay = jnp.dot(context_decay_low, decay_up, preferred_element_type=jnp.float32).astype(
        jnp.bfloat16
    )
    context_rate = jnp.dot(context_rate_low, rate_up, preferred_element_type=jnp.float32).astype(
        jnp.bfloat16
    )
    context_in = chain_inputs(context_keys, context_values, context_decay, context_rate, head_bias)
    latent_in = chain_inputs(keys, values, decay_pre, rate_pre, head_bias)
    rows = queries.shape[0]
    query_heads = queries.astype(jnp.float32).reshape(rows, -1, HEAD_DIM)
    forward_context_map = context_map(context_in, False)
    backward_context_map = context_map(context_in, True)
    forward_blocks = latent_blocks(query_heads, latent_in, False)
    backward_blocks = latent_blocks(query_heads, latent_in, True)
    heads = local // HEAD_DIM
    eye_heads = jnp.broadcast_to(jnp.eye(HEAD_DIM, dtype=jnp.float32), (heads, HEAD_DIM, HEAD_DIM))
    zero_heads = jnp.zeros((heads, HEAD_DIM, HEAD_DIM), jnp.float32)
    identity = (eye_heads, zero_heads)
    gathered = tuple(
        (
            part.astype(jnp.float32)
            for part in gather_packed(
                (
                    forward_context_map[0][None].astype(jnp.bfloat16),
                    forward_context_map[1][None].astype(jnp.bfloat16),
                    backward_context_map[0][None].astype(jnp.bfloat16),
                    backward_context_map[1][None].astype(jnp.bfloat16),
                ),
                "sp",
                (0, 0, 0, 0),
            )
        )
    )
    forward_context, _ = lax.scan(fold_state, zero_heads, (gathered[0], gathered[1]))
    backward_context, _ = lax.scan(fold_state, zero_heads, (gathered[2], gathered[3]), reverse=True)
    forward_entry = carried_in(forward_blocks[0], "sp", compose, identity, False)
    backward_entry = carried_in(backward_blocks[0], "sp", compose, identity, True)
    forward_start = product("hij,hjk->hik", forward_context, forward_entry[0]) + forward_entry[1]
    backward_start = (
        product("hij,hjk->hik", backward_context, backward_entry[0]) + backward_entry[1]
    )
    reads = latent_read(forward_start, forward_blocks, False) + latent_read(
        backward_start, backward_blocks, True
    )
    center = jnp.mean(reads, axis=-1, keepdims=True)
    variance = jnp.mean(jnp.square(reads - center), axis=-1, keepdims=True)
    normal_heads = ((reads - center) * lax.rsqrt(variance + GROUP_EPS)).reshape(rows, local)
    mixed = (normal_heads * group_gain * jax.nn.silu(branch.astype(jnp.float32))).astype(
        jnp.bfloat16
    )
    mixer = (
        summed_on_arrival(
            jnp.dot(mixed, out_weight, preferred_element_type=jnp.float32).astype(jnp.bfloat16),
            "tp",
            0,
        )
        .astype(jnp.bfloat16)
        .astype(jnp.float32)
    )
    normed_out = mixer * lax.rsqrt(jnp.mean(mixer * mixer, axis=-1, keepdims=True) + NORM_EPS)
    return (latent.astype(jnp.float32) + gate[0] * normed_out).astype(jnp.bfloat16)


def solution(mesh):
    placed = (
        P(("sp", "tp"), None),
        P("sp", None),
        P("sp"),
        P("sp"),
        P("sp", "tp"),
        P("sp", "tp"),
        P("sp", "tp"),
        P(),
        P(),
        P(None, "tp"),
        P(),
        P(None, "tp"),
        P(None, "tp"),
        P(None, "tp"),
        P(None, "tp"),
        P(None, "tp"),
        P(None, "tp"),
        P("tp"),
        P("tp", None),
    )
    return jax.shard_map(
        on_device, mesh=mesh, in_specs=placed, out_specs=P(("sp", "tp"), None), check_vma=False
    )
```

profile of v0, /device:TPU:1, one launch (start us, length us, event | category | flops | bytes accessed | tf_op | source)
XLA Modules:
  0.0 589.6 jit_solution(13339620628267169365)
XLA Ops:
  11.4 8.6 %all-to-all-start = ((f32[16,1,2560]{2,1,0:T(1,128)}), f32[16,1,2560]{2,1,0:T(1,128)S(1)}, u32[]{:S(2)}, u32[]{:S(2)}) async-start(f32[16,1,2560]{2,1,0:T(1,128)} %broadcast_in_dim.51), calls=%async_computation | async-start | bytes 327680 | tf_op jit(solution)/shard_map/all_to_all | solution.py:19
  27.2 15.0 %all_gather.9 = f32[5,4096]{1,0:T(8,128)S(1)} all-gather(f32[5,512]{1,0:T(8,128)S(1)} %pad_maximum_fusion.6), channel_id=1, replica_groups=mesh['sp'=16,'tp'=8] {'tp'}, dimensions={1}, use_global_device_ids=true | all-gather | bytes 92160 | tf_op jit(solution)/shard_map/all_gather | solution.py:37
  44.9 3.1 fusion.103
  48.2 3.2 convolution_convert_fusion.9
  55.5 4.0 all-to-all-start.1
  60.4 20.2 %custom-call.12 = f32[8,1,32,32]{2,3,1,0:T(8,128)S(1)} custom-call(f32[8,1,32,32]{3,2,1,0:T(8,128)S(1)} %fusion.89), custom_call_target="InvertDiagBlocksLowerTriangular" | custom-call | tf_op jit(solution)/shard_map/jit(_solve_triangular)/vmap()/triangular_solve | solution.py:158
  83.1 19.7 %custom-call.11 = f32[8,1,32,32]{2,3,1,0:T(8,128)S(1)} custom-call(f32[8,1,32,32]{3,2,1,0:T(8,128)S(1)} %fusion.86), custom_call_target="InvertDiagBlocksLowerTriangular" | custom-call | tf_op jit(solution)/shard_map/jit(_solve_triangular)/vmap()/triangular_solve | solution.py:158
  105.2 3.0 convolution_convert_fusion.2
  121.5 1.8 bitcast_multiply_fusion.5
  125.2 80.0 %custom-call.13 = f32[2,8,1,64,64]{3,4,2,1,0:T(8,128)} custom-call(f32[2,8,1,64,64]{4,3,2,1,0:T(8,128)} %fusion.46), custom_call_target="InvertDiagBlocksLowerTriangular" | custom-call | tf_op jit(solution)/shard_map/jit(_solve_triangular)/vmap(vmap())/triangular_solve | solution.py:158
  205.2 2.3 fusion.33
  207.5 2.5 fusion.130
  213.4 2.5 fusion.40
  215.9 2.2 fusion.43
  218.1 80.2 %custom-call.10 = f32[2,8,1,64,64]{3,4,2,1,0:T(8,128)} custom-call(f32[2,8,1,64,64]{4,3,2,1,0:T(8,128)} %fusion.43), custom_call_target="InvertDiagBlocksLowerTriangular" | custom-call | tf_op jit(solution)/shard_map/jit(_solve_triangular)/vmap(vmap())/triangular_solve | solution.py:158
  299.9 1.9 broadcast_in_dim.107
  301.7 4.6 reshape.575
  306.4 4.9 all-to-all-start.4
  311.3 2.5 fusion.125
  317.2 1.9 broadcast_in_dim.102
  319.1 4.6 reshape.571
  323.7 1.7 fusion.149
  328.5 5.3 all-to-all-start.2
  335.2 1.7 pad_add_fusion
  336.9 1.9 broadcast_in_dim.108
  338.8 4.6 reshape.573
  343.4 2.1 fusion.138
  345.4 3.6 fusion.66
  350.1 5.6 all-to-all-start.5
  355.7 2.4 convolution_add_fusion.11
  358.1 1.9 reshape_reshape.10
  360.1 1.8 copy.316
  363.9 1.9 broadcast_in_dim.104
  365.8 4.7 reshape.569
  370.5 1.8 rev.45
  372.3 2.1 reshape.534
  374.3 2.1 copy.317
  376.4 2.0 convolution_multiply_fusion.1
  378.4 2.4 fusion.41
  380.9 7.0 %all-to-all-start.3 = ((bf16[16,2,16384]{2,1,0:T(2,128)(2,1)}), bf16[16,2,16384]{2,1,0:T(2,128)(2,1)}, u32[]{:S(2)}, u32[]{:S(2)}) async-start(bf16[16,2,16384]{2,1,0:T(2,128)(2,1)} %reshape.569), calls=%async_computation.3 | async-start | bytes 2097152 | tf_op jit(solution)/shard_map/all_to_all | solution.py:19
  389.3 4.7 reshape.574
  394.0 2.3 convert_select_fusion
  396.3 1.5 slice.381
  400.4 4.7 reshape.576
  405.1 4.8 reshape.572
  409.9 4.8 convert_select_fusion.1
  417.2 2.3 slice.366
  419.5 4.8 reshape.570
  424.2 2.1 fusion.18
  434.8 5.0 reshape.561
  439.8 4.7 slice_convert_fusion
  444.5 3.2 reshape.555
  447.7 4.3 reshape.556
  452.0 36.8 %while.26 = (s32[]{:T(128)}, bf16[8,64,64]{1,2,0:T(8,128)(2,1)S(1)}, bf16[16,8,64,64]{3,2,1,0:T(8,128)(2,1)}, f32[16,8,64,64]{3,2,1,0:T(8,128)}, s32[]{:T(128)}, /*index=5*/s32[]{:T(128)}) while((s32[]{:T(128)}, bf16[8,64,64]{1,2,0:T(8,128)(2,1)S(1)}, bf16[16,8,64,64]{3,2,1,0:T(8,128)(2,1)}, f32[16,8,64,64]{3,2,1,0:T(8,128)}, ...), condition=%wide.region_6.9_spmd.clone, body=%wide.region_5.8_spmd.clone.sunk | while | flops 4292611 | bytes 1048671 | solution.py:331
  488.8 2.1 fusion.49
  493.4 2.3 convolution_add_fusion.9
  495.6 2.5 fusion.37
  500.6 3.2 reshape.559
  503.8 4.3 reshape.560
  508.1 36.8 %while.27 = (s32[]{:T(128)}, bf16[8,64,64]{1,2,0:T(8,128)(2,1)S(1)}, bf16[16,8,64,64]{3,2,1,0:T(8,128)(2,1)}, f32[16,8,64,64]{3,2,1,0:T(8,128)}, s32[]{:T(128)}, /*index=5*/s32[]{:T(128)}, s32[]{:T(128)}) while((s32[]{:T(128)}, bf16[8,64,64]{1,2,0:T(8,128)(2,1)S(1)}, bf16[16,8,64,64]{3,2,1,0:T(8,128)(2,1)}, ...), condition=%wide.region_8.11_spmd.clone, body=%wide.region_7.10_spmd.clone.sunk | while | flops 4292612 | bytes 1048691 | solution.py:332
  549.4 2.4 convolution_add_fusion.3
  551.8 1.4 fusion.32
  554.5 5.0 convolution_convert_fusion
  559.5 21.6 %all_to_all.36 = bf16[8,16,4096]{2,1,0:T(8,128)(2,1)S(1)} all-to-all(bf16[8,16,4096]{2,1,0:T(8,128)(2,1)S(1)} %bitcast.555), channel_id=1, replica_groups=mesh['sp'=16,'tp'=8] {'tp'}, dimensions={0} | all-to-all | bytes 2097152 | tf_op jit(solution)/shard_map/all_to_all | solution.py:102
  (442 shorter events, 153.6 us)
Async XLA Ops:
  6.5 36.4 %copy-start = (bf16[4096,128]{1,0:T(8,128)(2,1)S(1)}, bf16[4096,128]{1,0:T(8,128)(2,1)}, u32[]{:S(2)}) copy-start(bf16[4096,128]{1,0:T(8,128)(2,1)} %param.35) | copy-start | bytes 3145732
  6.5 36.4 %copy-start.26 = (bf16[32,4096]{1,0:T(8,128)(2,1)S(1)}, bf16[32,4096]{1,0:T(8,128)(2,1)}, u32[]{:S(2)}) copy-start(bf16[32,4096]{1,0:T(8,128)(2,1)} %param.28) | copy-start | bytes 786436
  6.5 36.4 %copy-start.50 = (f32[4096]{0:T(1024)S(1)}, f32[4096]{0:T(1024)}, u32[]{:S(2)}) copy-start(f32[4096]{0:T(1024)} %param.34) | copy-start | bytes 49156
  6.5 36.4 %copy-start.63 = (bf16[128,512]{1,0:T(8,128)(2,1)S(1)}, bf16[128,512]{1,0:T(8,128)(2,1)}, u32[]{:S(2)}) copy-start(bf16[128,512]{1,0:T(8,128)(2,1)} %param.36) | copy-start | bytes 393220
  11.4 15.6 %all-to-all-start = ((f32[16,1,2560]{2,1,0:T(1,128)}), f32[16,1,2560]{2,1,0:T(1,128)S(1)}, u32[]{:S(2)}, u32[]{:S(2)}) async-start(f32[16,1,2560]{2,1,0:T(1,128)} %broadcast_in_dim.51), calls=%async_computation | async-start | bytes 327680 | tf_op jit(solution)/shard_map/all_to_all | solution.py:19
  21.9 26.0 %copy-start.61 = (f32[1,512]{1,0:T(1,128)}, f32[1,512]{1,0:T(1,128)S(1)}, u32[]{:S(2)}) copy-start(f32[1,512]{1,0:T(1,128)S(1)} %get-tuple-element.226) | copy-start | bytes 6148
  21.9 30.9 %copy-start.59 = (f32[1,512]{1,0:T(1,128)}, f32[1,512]{1,0:T(1,128)S(1)}, u32[]{:S(2)}) copy-start(f32[1,512]{1,0:T(1,128)S(1)} %get-tuple-element.225) | copy-start | bytes 6148
  48.1 4.0 copy-start.39
  48.1 4.4 copy-start.42
  54.4 5.4 copy-start.49
  55.5 4.4 copy-start.46
  55.5 4.7 copy-start.51
  55.5 49.6 %all-to-all-start.1 = ((bf16[8,16,4352]{2,1,0:T(8,128)(2,1)}), bf16[8,16,4352]{2,1,0:T(8,128)(2,1)S(1)}, u32[]{:S(2)}, u32[]{:S(2)}) async-start(bf16[8,16,4352]{2,1,0:T(8,128)(2,1)} %broadcast_in_dim.52), calls=%async_computation.1 | async-start | bytes 2228224 | tf_op jit(solution)/shard_map/all_to_all | solution.py:19
  59.5 375.3 %all-gather.3.cloned.1.call-start = ((), (), s32[]{:S(2)}) async-start(), calls=%async_computation.7 | async-start | bytes 4456448 | tf_op jit(solution)/shard_map/all_gather | solution.py:56
  60.0 22.4 %copy-start.48 = (f32[1,32,8,64]{3,2,1,0:T(8,128)S(1)}, f32[1,32,8,64]{3,2,1,0:T(8,128)}, u32[]{:S(2)}) copy-start(f32[1,32,8,64]{3,2,1,0:T(8,128)} %reshape_reshape.24) | copy-start | bytes 196612
  105.1 3.1 copy-start.62
  105.1 3.1 copy-start.64
  105.2 3.5 copy-start.2
  108.7 1.0 copy-start.65
  111.7 3.5 copy-start.44
  120.7 84.4 %copy-start.15 = (f32[2,64,8,64]{3,1,2,0:T(8,128)}, f32[2,64,8,64]{3,1,2,0:T(8,128)S(1)}, u32[]{:S(2)}) copy-start(f32[2,64,8,64]{3,1,2,0:T(8,128)S(1)} %copy.323) | copy-start | bytes 786436
  120.9 3.2 copy-start.52
  121.4 88.6 %copy-start.6 = (f32[2,64,8,64]{3,1,2,0:T(8,128)}, f32[2,64,8,64]{3,1,2,0:T(8,128)S(1)}, u32[]{:S(2)}) copy-start(f32[2,64,8,64]{3,1,2,0:T(8,128)S(1)} %copy.322) | copy-start | bytes 786436
  121.4 2.6 copy-start.45
  121.5 2.6 copy-start.47
  210.0 3.1 copy-start.18
  210.0 2.0 copy-start.55
  210.1 1.9 copy-start.38
  210.4 3.0 copy-start.21
  210.4 2.8 copy-start.34
  213.4 142.3 %copy-start.4 = (f32[2,64,8,64]{3,1,2,0:T(8,128)}, f32[2,64,8,64]{3,1,2,0:T(8,128)S(1)}, u32[]{:S(2)}) copy-start(f32[2,64,8,64]{3,1,2,0:T(8,128)S(1)} %copy_multiply_fusion) | copy-start | bytes 786436
  306.4 22.2 %all-to-all-start.4 = ((bf16[16,2,16384]{2,1,0:T(2,128)(2,1)}), bf16[16,2,16384]{2,1,0:T(2,128)(2,1)}, u32[]{:S(2)}, u32[]{:S(2)}) async-start(bf16[16,2,16384]{2,1,0:T(2,128)(2,1)} %reshape.575), calls=%async_computation.4 | async-start | bytes 2097152 | tf_op jit(solution)/shard_map/all_to_all | solution.py:19
  311.3 3.3 copy-start.54
  323.7 1.7 copy-start.16
  323.7 1.7 copy-start.24
  328.5 21.5 %all-to-all-start.2 = ((bf16[16,2,16384]{2,1,0:T(2,128)(2,1)}), bf16[16,2,16384]{2,1,0:T(2,128)(2,1)}, u32[]{:S(2)}, u32[]{:S(2)}) async-start(bf16[16,2,16384]{2,1,0:T(2,128)(2,1)} %reshape.571), calls=%async_computation.2 | async-start | bytes 2097152 | tf_op jit(solution)/shard_map/all_to_all | solution.py:19
  350.1 30.8 %all-to-all-start.5 = ((bf16[16,2,16384]{2,1,0:T(2,128)(2,1)}), bf16[16,2,16384]{2,1,0:T(2,128)(2,1)}, u32[]{:S(2)}, u32[]{:S(2)}) async-start(bf16[16,2,16384]{2,1,0:T(2,128)(2,1)} %reshape.573), calls=%async_computation.5 | async-start | bytes 2097152 | tf_op jit(solution)/shard_map/all_to_all | solution.py:19
  358.1 5.0 slice-start
  365.8 10.6 %copy-start.7 = (f32[2,64,8,64]{3,1,2,0:T(8,128)S(1)}, f32[2,64,8,64]{3,1,2,0:T(8,128)}, u32[]{:S(2)}) copy-start(f32[2,64,8,64]{3,1,2,0:T(8,128)} %copy-done.6) | copy-start | bytes 786436
  378.4 9.5 %copy-start.29 = (f32[1,8,64,64]{3,2,1,0:T(8,128)S(1)}, f32[1,8,64,64]{3,2,1,0:T(8,128)}, u32[]{:S(2)}) copy-start(f32[1,8,64,64]{3,2,1,0:T(8,128)} %copy-done.28) | copy-start | bytes 393220
  378.4 9.5 %copy-start.32 = (f32[1,8,64,64]{3,2,1,0:T(8,128)S(1)}, f32[1,8,64,64]{3,2,1,0:T(8,128)}, u32[]{:S(2)}) copy-start(f32[1,8,64,64]{3,2,1,0:T(8,128)} %copy-done.31) | copy-start | bytes 393220
  380.9 7.8 %copy-start.27 = (f32[1,8,64,64]{3,2,1,0:T(8,128)S(1)}, f32[1,8,64,64]{3,2,1,0:T(8,128)}, u32[]{:S(2)}) copy-start(f32[1,8,64,64]{3,2,1,0:T(8,128)} %convolution_bitcast_fusion.8) | copy-start | bytes 393220
  380.9 7.8 %copy-start.30 = (f32[1,8,64,64]{3,2,1,0:T(8,128)S(1)}, f32[1,8,64,64]{3,2,1,0:T(8,128)}, u32[]{:S(2)}) copy-start(f32[1,8,64,64]{3,2,1,0:T(8,128)} %slice.427) | copy-start | bytes 393220
  380.9 38.6 %all-to-all-start.3 = ((bf16[16,2,16384]{2,1,0:T(2,128)(2,1)}), bf16[16,2,16384]{2,1,0:T(2,128)(2,1)}, u32[]{:S(2)}, u32[]{:S(2)}) async-start(bf16[16,2,16384]{2,1,0:T(2,128)(2,1)} %reshape.569), calls=%async_computation.3 | async-start | bytes 2097152 | tf_op jit(solution)/shard_map/all_to_all | solution.py:19
  387.9 6.1 %copy-start.58 = (pred[16]{0:T(512)(128)(4,1)S(1)}, pred[16]{0:T(512)(128)(4,1)}, u32[]{:S(2)}) copy-start(pred[16]{0:T(512)(128)(4,1)} %iota_compare_fusion.10) | copy-start | bytes 52
  405.1 4.8 copy-start.57
  414.7 1.4 copy-start.8
  424.2 2.6 copy-start.10
  426.9 2.7 copy-start.37
  426.9 1.7 copy-start.3
  429.0 1.6 copy-start.9
  429.0 1.9 copy-start.43
  431.4 1.6 copy-start.14
  488.8 3.5 copy-start.11
  490.9 4.7 copy-start.5
  498.1 2.4 copy-start.23
  508.1 40.3 %copy-start.12 = (f32[2,64,8,64]{3,1,2,0:T(8,128)S(1)}, f32[2,64,8,64]{3,1,2,0:T(8,128)}, u32[]{:S(2)}) copy-start(f32[2,64,8,64]{3,1,2,0:T(8,128)} %copy.317) | copy-start | bytes 786436
  544.9 4.5 copy-start.19
  548.3 3.5 copy-start.17
  548.3 3.5 copy-start.25
  553.3 1.2 copy-start.56
  554.5 27.7 %copy-start.1 = (bf16[4096,128]{1,0:T(8,128)(2,1)S(1)}, bf16[4096,128]{1,0:T(8,128)(2,1)}, u32[]{:S(2)}) copy-start(bf16[4096,128]{1,0:T(8,128)(2,1)} %param.35) | copy-start | bytes 3145732
  559.5 22.0 %copy-start.40 = (bf16[16,4096]{1,0:T(8,128)(2,1)S(1)}, bf16[16,4096]{1,0:T(8,128)(2,1)}, u32[]{:S(2)}) copy-start(bf16[16,4096]{1,0:T(8,128)(2,1)} %param.27) | copy-start | bytes 393220
  559.5 22.0 %copy-start.53 = (f32[1,4096]{1,0:T(1,128)S(1)}, f32[1,4096]{1,0:T(1,128)}, u32[]{:S(2)}) copy-start(f32[1,4096]{1,0:T(1,128)} %get-tuple-element.215) | copy-start | bytes 49156
  (10 other events, 8.3 us)
Sparse Core Ops, SparseCore 0:
  105.2 50.9 all-gather.2
where the time goes:
time: 597 us; the launch traced here: 590 us
  other arithmetic  227 us (38%)
  local copies, waits for them, and re-layouts  151 us (25%)
  matrix products  120 us (20%)
  blocking collectives  36.7 us (6%)
  starting transfers between devices  35.4 us (6%)
  between operations  15.3 us (3%)
    another operation x8, other arithmetic, block_terms(): jax.scipy.linalg.solve_triangular(system, right_side, lower=True, unit_di...  201 us
    dot_general x86, matrix products, product(): return jnp.einsum(form, left, right)  89.4 us
    unnamed x142, local copies, waits for them, and re-layouts  47.3 us
    all_to_all x6, starting transfers between devices, copy_for_each(): return lax.all_to_all(copies, axis, split_axis=0, concat_axis=0, tiled=True)  35.4 us
    dynamic_slice x64, local copies, waits for them, and re-layouts, on_device(): lax.scan(fold_state, zero_heads, (gathered[0], gathered[1]))  35.3 us
    all_to_all x1, blocking collectives, summed_on_arrival(): lax.all_to_all(in_blocks(value, dim, devices), axis, 0, 0, tiled=True)  21.6 us
    convert_element_type x4, local copies, waits for them, and re-layouts, on_device(): part.astype(jnp.float32)  15 us
    all_gather x1, blocking collectives, sent_together(): filled, at, outs = (lax.all_gather(both, axis, axis=dim, tiled=True), 0, [])  15 us
  transfers between devices with their start and end apart: 7, of which 3 were waited for; matrix products, arithmetic and copies ran while one was open for 59% of the time, Pallas kernels for 0%

commit v1 on v0

v1 whole, which is shorter than its diff:
```python
import functools
import math

import jax
import jax.numpy as jnp
from jax import lax
from jax.experimental import pallas as pl
from jax.experimental.pallas import tpu as pltpu
from jax.sharding import PartitionSpec as P

HEAD_DIM = 64
NORM_EPS = 1e-06
GROUP_EPS = 0.00064
DECAY_TOP = math.exp(-0.5)
MESH = pl.DeviceIdType.MESH
bf16 = jnp.bfloat16
f32 = jnp.float32
LEN = 128
N_SP = 16
N_TP = 8
HALF = 64


def mm(a, b):
    return jnp.dot(a, b, preferred_element_type=f32)


def mm_nt(a, b):
    return lax.dot_general(a, b, (((1,), (1,)), ((), ())), preferred_element_type=f32)


def split(a):
    high = a.astype(bf16)
    return high, (a - high.astype(f32)).astype(bf16)


def rows_cols():
    row = lax.broadcasted_iota(jnp.int32, (LEN, LEN), 0)
    col = lax.broadcasted_iota(jnp.int32, (LEN, LEN), 1)
    return row, col


def cumulative(log_decay, row, col):
    lower = jnp.where(row >= col, 1.0, 0.0).astype(bf16)
    high, low = split(log_decay)
    return mm(lower, high) + mm(lower, low)


def solve(couplings, sides, cross):
    row, col = rows_cols()
    eye = jnp.where(row == col, 1.0, 0.0)
    inverse = [eye + jnp.where(cross == 1, a, 0.0) for a in couplings]
    size = 2
    while size < LEN // 2:
        level = (cross >= size) & (cross < 2 * size)
        low = [d.astype(bf16) for d in inverse]
        part = [mm(jnp.where(level, a, 0.0).astype(bf16), d) for a, d in zip(couplings, low)]
        inverse = [d + mm(e, p.astype(bf16)) for d, e, p in zip(inverse, low, part)]
        size *= 2
    level = (cross >= size) & (cross < 2 * size)
    low = [d.astype(bf16) for d in inverse]
    first = [mm(d, s.astype(bf16)) for d, s in zip(low, sides)]
    part = [
        mm(jnp.where(level, a, 0.0).astype(bf16), y.astype(bf16)) for a, y in zip(couplings, first)
    ]
    return [y + mm(d, p.astype(bf16)) for y, d, p in zip(first, low, part)]


def head_mask(head):
    lane = lax.broadcasted_iota(jnp.int32, (1, LEN), 1)
    return (lane >= HALF) if head else (lane < HALF)


def pair_unit(keys):
    own = head_mask(0)
    square = keys * keys
    sums = [
        jnp.sum(jnp.where(mask, square, 0.0), axis=-1, keepdims=True)
        for mask in (own, head_mask(1))
    ]
    return keys * lax.rsqrt(jnp.where(own, sums[0], sums[1]) + 1.0)


def state_map(transposed, solved, crossed, total, head):
    lo = head * HALF
    out = mm(
        transposed[lo : lo + HALF], jnp.concatenate([solved, crossed], axis=0)
    )
    row = lax.broadcasted_iota(jnp.int32, (HALF, LEN), 0)
    lane = lax.broadcasted_iota(jnp.int32, (HALF, LEN), 1)
    out = out + jnp.where(lane == row + lo, jnp.exp(total), 0.0)
    return pltpu.roll(out, HALF, 1) if head else out


def pair_terms(queries, keys, values, log_decay, rate):
    row, col = rows_cols()
    cross = row ^ col
    cum = cumulative(log_decay, row, col)
    total = cum[LEN - 1 : LEN]
    half = 0.5 * total
    scale = jnp.exp(half)
    unit = pair_unit(keys)
    erase = -unit
    write = unit * rate
    before = jnp.exp(cum - log_decay - half)
    after = jnp.exp(half - cum)
    step = jnp.exp(log_decay)
    crossed_values = pltpu.roll(values, HALF, 1)
    own = [head_mask(0), head_mask(1)]
    units = []
    for direction in (0, 1):
        left, right = (before, after) if direction == 0 else (after, before)
        er, qr = erase * left, queries * (left * step)
        wr, kr = write * right, keys * right
        right_both = jnp.concatenate([wr, kr], axis=0).astype(bf16)
        transposed = jnp.concatenate(
            [jnp.transpose(wr * scale), jnp.transpose(kr * scale)], axis=1
        ).astype(bf16)
        for head in (0, 1):
            left_both = jnp.concatenate(
                [jnp.where(own[head], er, 0.0), jnp.where(own[head], qr, 0.0)], axis=0
            ).astype(bf16)
            grams = mm_nt(left_both, right_both)
            strict = (row > col) if direction == 0 else (row < col)
            reach = (row >= col) if direction == 0 else (row <= col)
            coupling = jnp.where(strict, grams[:LEN, :LEN], 0.0)
            feeding = jnp.where(strict, grams[:LEN, LEN:], 0.0).astype(bf16)
            attend = jnp.where(
                jnp.concatenate([reach, reach], axis=1), grams[LEN:], 0.0
            ).astype(bf16)
            fed = mm(feeding, crossed_values.astype(bf16))
            side = jnp.where(own[head], er, fed)
            units.append((direction, head, coupling, side, attend, qr, transposed))
    answers = solve([u[2] for u in units], [u[3] for u in units], cross)
    maps = [[None, None], [None, None]]
    reads = [[None, None], [None, None]]
    for unit_terms, answer in zip(units, answers):
        direction, head, _, _, attend, qr, transposed = unit_terms
        mine = own[head]
        solved = jnp.where(mine, answer * scale, answer).astype(bf16)
        crossed = jnp.where(mine, 0.0, crossed_values).astype(bf16)
        maps[direction][head] = state_map(transposed, solved, crossed, total, head)
        reads[direction][head] = mm(
            attend, jnp.concatenate([solved, crossed], axis=0)
        ) + jnp.where(mine, qr * scale, 0.0)
    ahead = [jnp.where(own[0], r[0], r[1]) for r in reads]
    local = jnp.where(own[0], reads[0][1], reads[0][0]) + jnp.where(
        own[0], reads[1][1], reads[1][0]
    )
    return jnp.concatenate(ahead, axis=1), pltpu.roll(local, HALF, 1), maps


def context_terms(pairs, lows, bias, backward):
    row, col = rows_cols()
    cross = row ^ col
    own = head_mask(0)
    order = (row - col) * (1 - 2 * backward)
    strict = order > 0
    units = []
    for pair, low in zip(pairs, lows):
        gates = jax.nn.sigmoid(bias + low)
        log_decay = jnp.where(own, -DECAY_TOP * gates, 0.0)
        rate = pltpu.roll(gates, HALF, 1)
        keys = jnp.where(own, pair, 0.0)
        cum = cumulative(log_decay, row, col)
        total = cum[LEN - 1 : LEN]
        half = 0.5 * total
        scale = jnp.exp(half)
        unit = keys * lax.rsqrt(jnp.sum(keys * keys, axis=-1, keepdims=True) + 1.0)
        one, two = cum - log_decay - half, half - cum
        left = jnp.exp(jnp.where(backward == 0, one, two))
        right = jnp.exp(jnp.where(backward == 0, two, one))
        er, wr, kr = -unit * left, unit * rate * right, keys * right
        grams = mm_nt(er.astype(bf16), jnp.concatenate([wr, kr], axis=0).astype(bf16))
        coupling = jnp.where(strict, grams[:, :LEN], 0.0)
        feeding = jnp.where(strict, grams[:, LEN:], 0.0).astype(bf16)
        crossed = jnp.where(own, 0.0, pair).astype(bf16)
        side = jnp.where(own, er, mm(feeding, crossed))
        transposed = jnp.concatenate(
            [jnp.transpose(wr * scale), jnp.transpose(kr * scale)], axis=1
        ).astype(bf16)
        units.append((coupling, side, transposed, crossed, scale, total))
    answers = solve([u[0] for u in units], [u[1] for u in units], cross)
    maps = []
    for (_, _, transposed, crossed, scale, total), answer in zip(units, answers):
        solved = jnp.where(own, answer * scale, answer).astype(bf16)
        maps.append(state_map(transposed, solved, crossed, total, 0))
    return maps


def advance(state, step_map):
    high, low = split(state)
    transfer = step_map[:, :HALF]
    return mm(transfer, high) + mm(transfer, low) + step_map.astype(f32)


def remote(src, dst, send, recv, sp, tp):
    return pltpu.make_async_remote_copy(
        src_ref=src,
        dst_ref=dst,
        send_sem=send,
        recv_sem=recv,
        device_id=(sp, tp),
        device_id_type=MESH,
    )


def kernel(
    latent,
    context,
    condition,
    context_condition,
    shift_weight,
    scale_weight,
    gate_weight,
    norm_gain,
    decay_down,
    decay_up,
    rate_down,
    rate_up,
    head_bias,
    query_weight,
    key_weight,
    value_weight,
    branch_weight,
    group_gain,
    out_weight,
    out,
    rows,
    own_rows,
    ctx_rows,
    cond,
    mod_w,
    gain,
    down,
    up,
    bias,
    wq,
    wk,
    wv,
    wb,
    ggain,
    wo,
    part,
    ybuf,
    zpart,
    zbuf,
    mods,
    normed,
    low,
    kbuf,
    vbuf,
    dbuf,
    rbuf,
    qbuf,
    bbuf,
    ctx_out,
    ctx_in,
    head_rows,
    map_out,
    map_in,
    ctx_maps,
    ahead,
    local,
    state_out,
    states,
    mixed,
    partial,
    paired,
    summed,
    arrived,
    load,
    y_s,
    y_r,
    z_s,
    z_r,
    t_s,
    t_r,
    l_s,
    l_r,
    f_s,
    c_s,
    c_r,
    m_s,
    m_r,
    s_s,
    s_r,
    o_s,
    o_r,
    g_s,
    g_r,
):
    sp = lax.axis_index("sp")
    tp = lax.axis_index("tp")
    zz, yy = sp // 4, sp % 4
    xx, core = tp // 2, tp % 2
    sibling = 2 * xx + (1 - core)
    width = wq.shape[1]
    model = normed.shape[1]
    blocks = model // width
    own_n = own_rows.shape[0]
    ctx_n = ctx_rows.shape[0]

    barrier = pltpu.get_barrier_semaphore()

    def greet_sp(j, carry):
        pl.semaphore_signal(
            barrier, inc=1, device_id=((sp + j) % N_SP, tp), device_id_type=MESH
        )
        return carry

    def greet_tp(j, carry):
        pl.semaphore_signal(
            barrier, inc=1, device_id=(sp, (tp + j) % N_TP), device_id_type=MESH
        )
        return carry

    lax.fori_loop(1, N_SP, greet_sp, 0)
    lax.fori_loop(1, N_TP, greet_tp, 0)

    def fetch(at, src, dst):
        return pltpu.make_async_copy(src, dst, load.at[at])

    copies = [
        fetch(0, condition, cond.at[0:1]),
        fetch(1, context_condition, cond.at[1:2]),
        fetch(2, shift_weight, mod_w.at[0]),
        fetch(3, scale_weight, mod_w.at[1]),
        fetch(4, gate_weight, mod_w.at[2]),
        fetch(5, latent, own_rows),
        fetch(6, context, ctx_rows),
        fetch(7, norm_gain, gain),
        fetch(8, decay_down, down.at[:, 0:LEN]),
        fetch(9, rate_down, down.at[:, LEN : 2 * LEN]),
        fetch(10, decay_up, up.at[0]),
        fetch(11, rate_up, up.at[1]),
        fetch(12, head_bias, bias),
        fetch(13, key_weight, wk),
        fetch(14, value_weight, wv),
        fetch(15, query_weight, wq),
        fetch(16, branch_weight, wb),
        fetch(17, group_gain, ggain),
        fetch(18, out_weight, wo),
    ]
    for copy in copies:
        copy.start()

    for at in (0, 1, 2, 3, 4):
        copies[at].wait()
    rows_c = cond[...]
    conditions = (rows_c * jax.nn.sigmoid(rows_c)).astype(bf16)
    conditions = jnp.concatenate([conditions, jnp.zeros((14, rows_c.shape[1]), bf16)], axis=0)
    shares = [mm(conditions, mod_w[at]) for at in range(3)]
    part[...] = jnp.concatenate(
        [shares[0][0:2], shares[1][0:2], shares[2][0:1], jnp.zeros((3, width), f32)], axis=0
    )
    ybuf[yy] = part[...]
    pl.semaphore_wait(barrier, N_SP - 1 + N_TP - 1)

    sends = []

    def start(copy):
        copy.start()
        sends.append(copy)

    for j in (1, 2, 3):
        to = zz * 4 + (yy + j) % 4
        start(remote(part, ybuf.at[yy], y_s.at[j], y_r.at[yy], to, tp))
    copies[5].wait()
    for j in (2, 1, 3):
        to = 2 * ((xx + j) % 4) + core
        start(remote(own_rows, rows.at[tp], l_s.at[j], l_r.at[tp], sp, to))
    start(remote(own_rows, rows.at[tp], l_s.at[0], l_r.at[tp], sp, sibling))
    rows[tp] = own_rows[...]

    for j in (1, 2, 3):
        frm = (yy + j) % 4
        remote(part, ybuf.at[frm], y_s.at[j], y_r.at[frm], sp, tp).wait_recv()
    zpart[...] = ybuf[0] + ybuf[1] + ybuf[2] + ybuf[3]
    zbuf[zz] = zpart[...]
    for j in (1, 2, 3):
        to = ((zz + j) % 4) * 4 + yy
        start(remote(zpart, zbuf.at[zz], z_s.at[j], z_r.at[zz], to, tp))

    copies[6].wait()
    ctx = ctx_rows[...].astype(f32)
    ctx_scale = lax.rsqrt(jnp.mean(ctx * ctx, axis=-1, keepdims=True) + NORM_EPS)

    for j in (1, 2, 3):
        frm = (zz + j) % 4
        remote(zpart, zbuf.at[frm], z_s.at[j], z_r.at[frm], sp, tp).wait_recv()
    part2 = zbuf[0] + zbuf[1] + zbuf[2] + zbuf[3]
    mods[tp] = part2
    for j in range(1, N_TP):
        to = (tp + j) % N_TP
        start(remote(mods.at[tp], mods.at[tp], t_s.at[j], t_r.at[tp], sp, to))

    for j in (1, 3, 2):
        frm = 2 * ((xx + j) % 4) + core
        remote(own_rows, rows.at[frm], l_s.at[j], l_r.at[frm], sp, tp).wait_recv()
        start(remote(rows.at[frm], rows.at[frm], f_s.at[j], l_r.at[frm], sp, sibling))
    for j in (0, 1, 3, 2):
        frm = 2 * ((xx + j) % 4) + (1 - core)
        remote(own_rows, rows.at[frm], l_s.at[j], l_r.at[frm], sp, tp).wait_recv()
    inverses = []
    for i in range(N_TP):
        values = rows[i].astype(f32)
        inverses.append(lax.rsqrt(jnp.mean(values * values, axis=-1, keepdims=True) + NORM_EPS))

    copies[7].wait()
    for j in range(1, N_TP):
        frm = (tp + j) % N_TP
        remote(part, mods.at[frm], t_s.at[j], t_r.at[frm], sp, tp).wait_recv()

    for j in range(blocks):
        cols = slice(j * width, (j + 1) * width)
        vectors = mods[j]
        factor = gain[0:1, cols] * (1.0 + vectors[2:3])
        shift = vectors[0:1]
        for i in range(N_TP):
            normed[i * own_n : (i + 1) * own_n, cols] = (
                rows[i, :, cols].astype(f32) * inverses[i] * factor + shift
            ).astype(bf16)
        factor = gain[0:1, cols] * (1.0 + vectors[3:4])
        shift = vectors[1:2]
        normed[LEN : LEN + ctx_n, cols] = (
            ctx_rows[:, cols].astype(f32) * ctx_scale * factor + shift
        ).astype(bf16)

    for at in (8, 9, 10, 11, 12):
        copies[at].wait()
    lows = mm(normed[...], down[...])
    low[:, :LEN] = jnp.tanh(lows[:, :LEN]).astype(bf16)
    low[:, LEN:] = lows[:, LEN:].astype(bf16)
    dbuf[...] = mm(low[:, :LEN], up[0]).astype(bf16)
    rbuf[...] = mm(low[:, LEN:], up[1]).astype(bf16)

    def project(weight, to, count):
        def body(i, carry):
            at = pl.ds(pl.multiple_of(i * 256, 256), 256)
            to[:, at] = mm(normed[0:count], weight[:, at]).astype(bf16)
            return carry

        lax.fori_loop(0, width // 256, body, 0)

    copies[13].wait()
    project(wk, kbuf, LEN + ctx_n)
    copies[14].wait()
    project(wv, vbuf, LEN + ctx_n)

    lane = lax.broadcasted_iota(jnp.int32, (1, LEN), 1)
    left = lane < HALF
    for p in range(width // LEN):
        cols = slice(p * LEN, (p + 1) * LEN)
        for at, (first, second) in enumerate(((kbuf, vbuf), (dbuf, rbuf))):
            a = first[LEN : LEN + ctx_n, cols].astype(f32)
            b = second[LEN : LEN + ctx_n, cols].astype(f32)
            lanes = slice(at * LEN, (at + 1) * LEN)
            ctx_out[2 * p, :, lanes] = jnp.where(left, a, pltpu.roll(b, HALF, 1)).astype(bf16)
            ctx_out[2 * p + 1, :, lanes] = jnp.where(left, pltpu.roll(a, HALF, 1), b).astype(bf16)
        a = bias[0:1, cols]
        b = bias[1:2, cols]
        head_rows[2 * p : 2 * p + 1] = jnp.where(left, a, pltpu.roll(b, HALF, 1))
        head_rows[2 * p + 1 : 2 * p + 2] = jnp.where(left, pltpu.roll(a, HALF, 1), b)
    my_head = sp % 8
    backward = sp // 8
    ctx_in[sp] = ctx_out[my_head]

    def send_ctx(j, carry):
        to = (sp + j) % N_SP
        remote(ctx_out.at[to % 8], ctx_in.at[sp], c_s.at[j], c_r.at[sp], to, tp).start()
        return carry

    lax.fori_loop(1, N_SP, send_ctx, 0)

    copies[15].wait()
    project(wq, qbuf, LEN)
    copies[16].wait()
    project(wb, bbuf, LEN)

    def map_copy(to, carry=None):
        return remote(map_out.at[to], map_in.at[sp], m_s.at[to], m_r.at[sp], to, tp)

    def chunk(p, carry):
        at = pl.ds(pl.multiple_of(p * LEN, LEN), LEN)
        gates = jax.nn.sigmoid(bias[0:1, at] + dbuf[0:LEN, at].astype(f32))
        rate = jax.nn.sigmoid(bias[1:2, at] + rbuf[0:LEN, at].astype(f32))
        coming, here, maps = pair_terms(
            qbuf[:, at].astype(f32),
            kbuf[0:LEN, at].astype(f32),
            vbuf[0:LEN, at].astype(f32),
            -DECAY_TOP * gates,
            rate,
        )
        for direction in (0, 1):
            for head in (0, 1):
                map_out[direction * 8 + 2 * p + head] = maps[direction][head].astype(bf16)
        for direction in (0, 1):
            for head in (0, 1):
                to = direction * 8 + 2 * p + head

                @pl.when(to != sp)
                def _():
                    map_copy(to).start()

        ahead[p] = coming.astype(bf16)
        local[p] = here
        return carry

    lax.fori_loop(0, width // LEN, chunk, 0)
    map_in[sp] = map_out[sp]

    for j in range(1, N_SP):
        frm = (sp + j) % N_SP
        remote(ctx_out.at[0], ctx_in.at[frm], c_s.at[j], c_r.at[frm], sp, tp).wait_recv()
    my_bias = head_rows[pl.ds(my_head, 1)]
    per = LEN // ctx_n
    pairs, lows_in = [], []
    for c in range(N_SP // per):
        pairs.append(ctx_in[c * per : (c + 1) * per, :, 0:LEN].astype(f32).reshape(LEN, LEN))
        lows_in.append(ctx_in[c * per : (c + 1) * per, :, LEN:].astype(f32).reshape(LEN, LEN))
    for c, found in enumerate(context_terms(pairs, lows_in, my_bias, backward)):
        ctx_maps[c] = found
    count = N_SP // per
    forward = backward == 0
    state = ctx_maps[jnp.where(forward, 0, count - 1)]
    for c in range(1, count):
        state = advance(state, ctx_maps[jnp.where(forward, c, count - 1 - c)].astype(bf16))

    odd = my_head % 2
    keep = (lane >= HALF) == (odd == 1)

    def walk(i, state):
        at = jnp.where(forward, i, N_SP - 1 - i)
        shown = jnp.where(odd == 1, state, pltpu.roll(state, HALF, 1))
        state_out[at] = jnp.where(keep, shown, 0.0).astype(bf16)

        @pl.when(at != sp)
        def _():
            remote(state_out.at[at], states.at[sp], s_s.at[at], s_r.at[sp], at, tp).start()
            remote(map_out.at[0], map_in.at[at], m_s.at[at], m_r.at[at], sp, tp).wait_recv()

        return advance(state, map_in[at])

    lax.fori_loop(0, N_SP, walk, state)
    states[sp] = state_out[sp]
    for j in range(1, N_SP):
        frm = (sp + j) % N_SP
        remote(state_out.at[0], states.at[frm], s_s.at[0], s_r.at[frm], sp, tp).wait_recv()

    copies[17].wait()
    other = lane >= HALF
    for p in range(width // LEN):
        cols = slice(p * LEN, (p + 1) * LEN)
        both = jnp.concatenate(
            [
                states[2 * p : 2 * p + 2].reshape(LEN, LEN),
                states[8 + 2 * p : 8 + 2 * p + 2].reshape(LEN, LEN),
            ],
            axis=0,
        )
        reads = mm(ahead[p], both) + local[p]

        def head_mean(x):
            sums = [
                jnp.sum(jnp.where(mask, x, 0.0), axis=-1, keepdims=True) for mask in (left, other)
            ]
            return jnp.where(left, sums[0], sums[1]) * (1.0 / HALF)

        centred = reads - head_mean(reads)
        normal = centred * lax.rsqrt(head_mean(centred * centred) + GROUP_EPS)
        gate = bbuf[:, cols].astype(f32)
        mixed[:, cols] = (
            normal * ggain[0:1, cols] * (gate * jax.nn.sigmoid(gate))
        ).astype(bf16)

    copies[18].wait()
    n_chunk = arrived.shape[0]
    piece = model // n_chunk
    for c in range(n_chunk):
        cols = slice(c * piece, (c + 1) * piece)
        product = mm(mixed[...], wo[:, cols]).astype(bf16)
        for x in range(4):
            for k in range(2):
                lo = (2 * x + k) * own_n
                partial[c, k, x] = product[lo : lo + own_n]
        start(
            remote(
                partial.at[c, 1 - core], paired.at[c], o_s.at[c], o_r.at[c], sp, sibling
            )
        )
    for c in range(n_chunk):
        remote(partial.at[c, 0], paired.at[c], o_s.at[c], o_r.at[c], sp, tp).wait_recv()
        summed[c] = (partial[c, core].astype(f32) + paired[c].astype(f32)).astype(bf16)
        for j in (2, 1, 3):
            x = (xx + j) % 4
            start(
                remote(
                    summed.at[c, x], arrived.at[c, xx], g_s.at[c, j], g_r.at[c, xx], sp, 2 * x + core
                )
            )
        arrived[c, xx] = summed[c, xx]
    pieces = []
    for c in range(n_chunk):
        for j in (1, 3, 2):
            x = (xx + j) % 4
            remote(
                summed.at[c, 0], arrived.at[c, x], g_s.at[c, j], g_r.at[c, x], sp, tp
            ).wait_recv()
        total = arrived[c, 0].astype(f32)
        for x in range(1, 4):
            total = total + arrived[c, x].astype(f32)
        pieces.append(total.astype(bf16).astype(f32))
    square = sum(jnp.sum(p * p, axis=-1, keepdims=True) for p in pieces)
    inverse = lax.rsqrt(square * (1.0 / model) + NORM_EPS)
    for c in range(n_chunk):
        for s in range(piece // width):
            j = c * (piece // width) + s
            cols = slice(j * width, (j + 1) * width)
            value = pieces[c][:, s * width : (s + 1) * width]
            out[:, cols] = (
                own_rows[:, cols].astype(f32) + mods[j, 4:5] * (value * inverse)
            ).astype(bf16)

    for copy in sends:
        copy.wait_send()

    def drain_ctx(j, carry):
        remote(ctx_out.at[0], ctx_in.at[0], c_s.at[j], c_r.at[0], sp, tp).wait_send()
        to = (sp + j) % N_SP
        remote(map_out.at[0], map_in.at[0], m_s.at[to], m_r.at[0], sp, tp).wait_send()
        remote(state_out.at[0], states.at[0], s_s.at[to], s_r.at[0], sp, tp).wait_send()
        return carry

    lax.fori_loop(1, N_SP, drain_ctx, 0)


def on_device(
    latent,
    context,
    condition,
    context_condition,
    shift_weight,
    scale_weight,
    gate_weight,
    norm_gain,
    decay_down,
    decay_up,
    rate_down,
    rate_up,
    head_bias,
    query_weight,
    key_weight,
    value_weight,
    branch_weight,
    group_gain,
    out_weight,
):
    own_n, model = latent.shape
    ctx_n = context.shape[0]
    width = query_weight.shape[1]
    held = condition.shape[0]
    args = (
        latent,
        context,
        condition.reshape(1, -1),
        context_condition.reshape(1, -1),
        shift_weight,
        scale_weight,
        gate_weight,
        norm_gain.reshape(1, -1),
        decay_down,
        decay_up,
        rate_down,
        rate_up,
        head_bias,
        query_weight,
        key_weight,
        value_weight,
        branch_weight,
        group_gain.reshape(1, -1),
        out_weight,
    )
    n_chunk = 4
    piece = model // n_chunk
    V = pltpu.VMEM
    dma = pltpu.SemaphoreType.DMA
    scratch = [
        V((N_TP, own_n, model), bf16),
        V((own_n, model), bf16),
        V((ctx_n, model), bf16),
        V((2, held), f32),
        V((3, held, width), bf16),
        V((1, model), f32),
        V((model, 2 * LEN), bf16),
        V((2, LEN, width), bf16),
        V((2, width), f32),
        V((model, width), bf16),
        V((model, width), bf16),
        V((model, width), bf16),
        V((model, width), bf16),
        V((1, width), f32),
        V((width, model), bf16),
        V((8, width), f32),
        V((4, 8, width), f32),
        V((8, width), f32),
        V((4, 8, width), f32),
        V((N_TP, 8, width), f32),
        V((LEN + ctx_n, model), bf16),
        V((LEN + ctx_n, 2 * LEN), bf16),
        V((LEN + ctx_n, width), bf16),
        V((LEN + ctx_n, width), bf16),
        V((LEN + ctx_n, width), bf16),
        V((LEN + ctx_n, width), bf16),
        V((LEN, width), bf16),
        V((LEN, width), bf16),
        V((8, ctx_n, 2 * LEN), bf16),
        V((N_SP, ctx_n, 2 * LEN), bf16),
        V((8, LEN), f32),
        V((N_SP, HALF, LEN), bf16),
        V((N_SP, HALF, LEN), bf16),
        V((4, HALF, LEN), f32),
        V((width // LEN, LEN, 2 * LEN), bf16),
        V((width // LEN, LEN, LEN), f32),
        V((N_SP, HALF, LEN), bf16),
        V((N_SP, HALF, LEN), bf16),
        V((LEN, width), bf16),
        V((n_chunk, 2, 4, own_n, piece), bf16),
        V((n_chunk, 4, own_n, piece), bf16),
        V((n_chunk, 4, own_n, piece), bf16),
        V((n_chunk, 4, own_n, piece), bf16),
        dma((19,)),
        dma((4,)),
        dma((4,)),
        dma((4,)),
        dma((4,)),
        dma((N_TP,)),
        dma((N_TP,)),
        dma((4,)),
        dma((N_TP,)),
        dma((4,)),
        dma((N_SP,)),
        dma((N_SP,)),
        dma((N_SP,)),
        dma((N_SP,)),
        dma((N_SP,)),
        dma((N_SP,)),
        dma((n_chunk,)),
        dma((n_chunk,)),
        dma((n_chunk, 4)),
        dma((n_chunk, 4)),
    ]
    return pl.pallas_call(
        kernel,
        out_shape=jax.ShapeDtypeStruct((own_n, model), bf16),
        in_specs=[pl.BlockSpec(memory_space=pl.ANY)] * len(args),
        out_specs=pl.BlockSpec(memory_space=pltpu.VMEM),
        scratch_shapes=scratch,
        compiler_params=pltpu.CompilerParams(
            collective_id=0, has_side_effects=True, vmem_limit_bytes=60 * 1024 * 1024
        ),
    )(*args)


def solution(mesh):
    placed = (
        P(("sp", "tp"), None),
        P("sp", None),
        P("sp"),
        P("sp"),
        P("sp", "tp"),
        P("sp", "tp"),
        P("sp", "tp"),
        P(),
        P(),
        P(None, "tp"),
        P(),
        P(None, "tp"),
        P(None, "tp"),
        P(None, "tp"),
        P(None, "tp"),
        P(None, "tp"),
        P(None, "tp"),
        P("tp"),
        P("tp", None),
    )
    return jax.shard_map(
        on_device, mesh=mesh, in_specs=placed, out_specs=P(("sp", "tp"), None), check_vma=False
    )
```

time: 597 us -> 63.3 us (0.11); the launches traced: 590 us -> 63.1 us
  other arithmetic: 227 us -> 0 us
  local copies, waits for them, and re-layouts: 151 us -> 1.57 us
  matrix products: 120 us -> 0 us
  Pallas kernels: 0 us -> 61.6 us
  blocking collectives: 36.7 us -> 0 us
  starting transfers between devices: 35.4 us -> 0 us
  between operations: 15.3 us -> 0.01 us
    another operation x8 -> x0, other arithmetic: 201 us -> none  [block_terms(): jax.scipy.linalg.solve_triangular(system, right_side, lower=True, unit_di...]
    dot_general x101 -> x0, matrix products: 114 us -> none  [the longest x86 89.4 us: product(): return jnp.einsum(form, left, right)]
    pallas_call x0 -> x1, Pallas kernels: none -> 61.6 us  [on_device(): pl.pallas_call(kernel, out_shape=jax.ShapeDtypeStruct((own_n, model), bf1...]
    unnamed x142 -> x1, local copies, waits for them, and re-layouts: 47.3 us -> 1.57 us
    all_to_all x6 -> x0, starting transfers between devices: 35.4 us -> none  [copy_for_each(): return lax.all_to_all(copies, axis, split_axis=0, concat_axis=0, tiled=True)]
    dynamic_slice x64 -> x0, local copies, waits for them, and re-layouts: 35.3 us -> none  [on_device(): lax.scan(fold_state, zero_heads, (gathered[0], gathered[1]))]
    all_to_all x1 -> x0, blocking collectives: 21.6 us -> none  [summed_on_arrival(): lax.all_to_all(in_blocks(value, dim, devices), axis, 0, 0, tiled=True)]
    convert_element_type x6 -> x0, local copies, waits for them, and re-layouts: 17 us -> none  [the longest x4 15 us: on_device(): part.astype(jnp.float32)]
  transfers between devices with their start and end apart: 7 -> 0, of which waited for: 3 -> 0; matrix products, arithmetic and copies ran while one was open for 59% -> 0% of each run, Pallas kernels for 0% -> 0%
where the time goes in v1:
time: 63.3 us; the launch traced here: 63.1 us
  Pallas kernels  61.6 us (97%)
  local copies, waits for them, and re-layouts  1.57 us (2%)
    pallas_call x1, Pallas kernels, on_device(): pl.pallas_call(kernel, out_shape=jax.ShapeDtypeStruct((own_n, model), bf1...  61.6 us
    unnamed x1, local copies, waits for them, and re-layouts  1.57 us

profile of v1, /device:TPU:1, one launch (start us, length us, event | category | flops | bytes accessed | tf_op | source)
XLA Modules:
  0.0 63.1 jit_solution(16713955968977736974)
XLA Ops:
  0.0 61.6 %shard_map.181 = bf16[16,4096]{1,0:T(8,128)(2,1)} custom-call(bf16[16,4096]{1,0:T(8,128)(2,1)} %latent.1, bf16[32,4096]{1,0:T(8,128)(2,1)} %context.1, f32[1,256]{1,0:T(1,128)} %bitcast.6, f32[1,256]{1,0:T(1,128)} %bitcast.7, bf16[256,512]{1,0:T(8,128)(2,1)} %shift_weight.1, bf16[256,512]{1,0:T(8,128)(2,1)} %scale_weight.1, bf16[256,512]{1,0:T(8,128)(2,1)} %gate_weight.1, ...), custom_call_target="tpu_custom_call" | custom-call | tf_op jit(solution)/shard_map/pallas_call | solution.py:753
  61.6 1.6 %copy.21 = bf16[16,4096]{1,0:T(8,128)(2,1)} copy(bf16[16,4096]{1,0:T(8,128)(2,1)} %shard_map.181) | data formatting | bytes 262144

commit v2 on v1

--- a/solution.py
+++ b/solution.py
@@ -1,4 +1,4 @@
-import functools
+import contextlib
 import math
 
 import jax
@@ -16,6 +16,8 @@
 bf16 = jnp.bfloat16
 f32 = jnp.float32
 LEN = 128
+group = 2
+lag = 5
 N_SP = 16
 N_TP = 8
 HALF = 64
@@ -92,9 +94,7 @@
     return pltpu.roll(out, HALF, 1) if head else out
 
 
-def pair_terms(queries, keys, values, log_decay, rate):
-    row, col = rows_cols()
-    cross = row ^ col
+def pair_setup(keys, values, log_decay, rate, row, col):
     cum = cumulative(log_decay, row, col)
     total = cum[LEN - 1 : LEN]
     half = 0.5 * total
@@ -106,48 +106,72 @@
     after = jnp.exp(half - cum)
     step = jnp.exp(log_decay)
     crossed_values = pltpu.roll(values, HALF, 1)
+    fed_by = crossed_values.astype(bf16)
     own = [head_mask(0), head_mask(1)]
-    units = []
+    units, rights, factors = [], [], []
     for direction in (0, 1):
         left, right = (before, after) if direction == 0 else (after, before)
-        er, qr = erase * left, queries * (left * step)
+        er = erase * left
         wr, kr = write * right, keys * right
         right_both = jnp.concatenate([wr, kr], axis=0).astype(bf16)
+        rights.append(right_both)
+        factors.append(left * step)
         transposed = jnp.concatenate(
             [jnp.transpose(wr * scale), jnp.transpose(kr * scale)], axis=1
         ).astype(bf16)
+        left_both = jnp.concatenate([jnp.where(mask, er, 0.0) for mask in own], axis=0)
+        grams = mm_nt(left_both.astype(bf16), right_both)
+        strict = (row > col) if direction == 0 else (row < col)
         for head in (0, 1):
-            left_both = jnp.concatenate(
-                [jnp.where(own[head], er, 0.0), jnp.where(own[head], qr, 0.0)], axis=0
-            ).astype(bf16)
-            grams = mm_nt(left_both, right_both)
-            strict = (row > col) if direction == 0 else (row < col)
-            reach = (row >= col) if direction == 0 else (row <= col)
-            coupling = jnp.where(strict, grams[:LEN, :LEN], 0.0)
-            feeding = jnp.where(strict, grams[:LEN, LEN:], 0.0).astype(bf16)
-            attend = jnp.where(
-                jnp.concatenate([reach, reach], axis=1), grams[LEN:], 0.0
-            ).astype(bf16)
-            fed = mm(feeding, crossed_values.astype(bf16))
-            side = jnp.where(own[head], er, fed)
-            units.append((direction, head, coupling, side, attend, qr, transposed))
-    answers = solve([u[2] for u in units], [u[3] for u in units], cross)
-    maps = [[None, None], [None, None]]
-    reads = [[None, None], [None, None]]
-    for unit_terms, answer in zip(units, answers):
-        direction, head, _, _, attend, qr, transposed = unit_terms
-        mine = own[head]
-        solved = jnp.where(mine, answer * scale, answer).astype(bf16)
-        crossed = jnp.where(mine, 0.0, crossed_values).astype(bf16)
-        maps[direction][head] = state_map(transposed, solved, crossed, total, head)
-        reads[direction][head] = mm(
-            attend, jnp.concatenate([solved, crossed], axis=0)
-        ) + jnp.where(mine, qr * scale, 0.0)
-    ahead = [jnp.where(own[0], r[0], r[1]) for r in reads]
-    local = jnp.where(own[0], reads[0][1], reads[0][0]) + jnp.where(
-        own[0], reads[1][1], reads[1][0]
-    )
-    return jnp.concatenate(ahead, axis=1), pltpu.roll(local, HALF, 1), maps
+            rows = slice(head * LEN, (head + 1) * LEN)
+            coupling = jnp.where(strict, grams[rows, :LEN], 0.0)
+            feeding = jnp.where(strict, grams[rows, LEN:], 0.0).astype(bf16)
+            side = jnp.where(own[head], er, mm(feeding, fed_by))
+            units.append((coupling, side, transposed, head))
+    return units, rights, factors, crossed_values, scale, total
+
+
+def pairs_terms(inputs):
+    row, col = rows_cols()
+    setups = [pair_setup(*given, row, col) for given in inputs]
+    flat = [unit for setup in setups for unit in setup[0]]
+    answers = solve([u[0] for u in flat], [u[1] for u in flat], row ^ col)
+    results, at = [], 0
+    for units, rights, factors, crossed_values, scale, total in setups:
+        maps, solved = [], []
+        for _, _, transposed, head in units:
+            mine = head_mask(head)
+            answer = answers[at]
+            at += 1
+            rows = jnp.where(mine, answer * scale, answer).astype(bf16)
+            crossed = jnp.where(mine, 0.0, crossed_values).astype(bf16)
+            maps.append(state_map(transposed, rows, crossed, total, head))
+            solved.append(rows)
+        results.append((maps, solved, rights, factors, scale))
+    return results
+
+
+def pair_reads(queries, values, solved, rights, factors, scale):
+    row, col = rows_cols()
+    own = [head_mask(0), head_mask(1)]
+    crossed_values = pltpu.roll(values, HALF, 1)
+    crossed = [jnp.where(mask, 0.0, crossed_values).astype(bf16) for mask in own]
+    reads = []
+    for direction in (0, 1):
+        qr = queries * factors[direction]
+        left_both = jnp.concatenate([jnp.where(mask, qr, 0.0) for mask in own], axis=0)
+        grams = mm_nt(left_both.astype(bf16), rights[direction])
+        reach = (row >= col) if direction == 0 else (row <= col)
+        both = jnp.concatenate([reach, reach], axis=1)
+        for head in (0, 1):
+            attend = jnp.where(both, grams[head * LEN : (head + 1) * LEN], 0.0).astype(bf16)
+            reads.append(
+                mm(attend, jnp.concatenate([solved[2 * direction + head], crossed[head]], axis=0))
+                + jnp.where(own[head], qr * scale, 0.0)
+            )
+    ahead = [jnp.where(own[0], reads[at], reads[at + 1]) for at in (0, 2)]
+    local = jnp.where(own[0], reads[1], reads[0]) + jnp.where(own[0], reads[3], reads[2])
+    return jnp.concatenate(ahead, axis=1), pltpu.roll(local, HALF, 1)
 
 
 def context_terms(pairs, lows, bias, backward):
@@ -188,10 +212,11 @@
     return maps
 
 
-def advance(state, step_map):
-    high, low = split(state)
-    transfer = step_map[:, :HALF]
-    return mm(transfer, high) + mm(transfer, low) + step_map.astype(f32)
+def compose(earlier, later):
+    high, low = split(earlier)
+    transfer = later[:, :HALF].astype(bf16)
+    lane = lax.broadcasted_iota(jnp.int32, (1, LEN), 1)
+    return mm(transfer, high) + mm(transfer, low) + jnp.where(lane >= HALF, later, 0.0)
 
 
 def remote(src, dst, send, recv, sp, tp):
@@ -260,6 +285,10 @@
     map_out,
     map_in,
     ctx_maps,
+    solved_buf,
+    right_buf,
+    factor_buf,
+    scale_buf,
     ahead,
     local,
     state_out,
@@ -301,6 +330,13 @@
     own_n = own_rows.shape[0]
     ctx_n = ctx_rows.shape[0]
 
+    scopes = contextlib.ExitStack()
+
+    def phase(name):
+        scopes.close()
+        scopes.enter_context(jax.named_scope(name))
+
+    phase("greet")
     barrier = pltpu.get_barrier_semaphore()
 
     def greet_sp(j, carry):
@@ -345,8 +381,10 @@
     for copy in copies:
         copy.start()
 
+    phase("wait_mod_w")
     for at in (0, 1, 2, 3, 4):
         copies[at].wait()
+    phase("shares")
     rows_c = cond[...]
     conditions = (rows_c * jax.nn.sigmoid(rows_c)).astype(bf16)
     conditions = jnp.concatenate([conditions, jnp.zeros((14, rows_c.shape[1]), bf16)], axis=0)
@@ -355,8 +393,10 @@
         [shares[0][0:2], shares[1][0:2], shares[2][0:1], jnp.zeros((3, width), f32)], axis=0
     )
     ybuf[yy] = part[...]
+    phase("barrier")
     pl.semaphore_wait(barrier, N_SP - 1 + N_TP - 1)
 
+    phase("send_y")
     sends = []
 
     def start(copy):
@@ -373,6 +413,7 @@
     start(remote(own_rows, rows.at[tp], l_s.at[0], l_r.at[tp], sp, sibling))
     rows[tp] = own_rows[...]
 
+    phase("wait_y")
     for j in (1, 2, 3):
         frm = (yy + j) % 4
         remote(part, ybuf.at[frm], y_s.at[j], y_r.at[frm], sp, tp).wait_recv()
@@ -382,10 +423,12 @@
         to = ((zz + j) % 4) * 4 + yy
         start(remote(zpart, zbuf.at[zz], z_s.at[j], z_r.at[zz], to, tp))
 
+    phase("ctx_stats")
     copies[6].wait()
     ctx = ctx_rows[...].astype(f32)
     ctx_scale = lax.rsqrt(jnp.mean(ctx * ctx, axis=-1, keepdims=True) + NORM_EPS)
 
+    phase("wait_z")
     for j in (1, 2, 3):
         frm = (zz + j) % 4
         remote(zpart, zbuf.at[frm], z_s.at[j], z_r.at[frm], sp, tp).wait_recv()
@@ -395,23 +438,28 @@
         to = (tp + j) % N_TP
         start(remote(mods.at[tp], mods.at[tp], t_s.at[j], t_r.at[tp], sp, to))
 
+    phase("latent_x")
     for j in (1, 3, 2):
         frm = 2 * ((xx + j) % 4) + core
         remote(own_rows, rows.at[frm], l_s.at[j], l_r.at[frm], sp, tp).wait_recv()
         start(remote(rows.at[frm], rows.at[frm], f_s.at[j], l_r.at[frm], sp, sibling))
+    phase("latent_core")
     for j in (0, 1, 3, 2):
         frm = 2 * ((xx + j) % 4) + (1 - core)
         remote(own_rows, rows.at[frm], l_s.at[j], l_r.at[frm], sp, tp).wait_recv()
+    phase("latent_stats")
     inverses = []
     for i in range(N_TP):
         values = rows[i].astype(f32)
         inverses.append(lax.rsqrt(jnp.mean(values * values, axis=-1, keepdims=True) + NORM_EPS))
 
+    phase("wait_t")
     copies[7].wait()
     for j in range(1, N_TP):
         frm = (tp + j) % N_TP
         remote(part, mods.at[frm], t_s.at[j], t_r.at[frm], sp, tp).wait_recv()
 
+    phase("normalize")
     for j in range(blocks):
         cols = slice(j * width, (j + 1) * width)
         vectors = mods[j]
@@ -427,6 +475,7 @@
             ctx_rows[:, cols].astype(f32) * ctx_scale * factor + shift
         ).astype(bf16)
 
+    phase("lows")
     for at in (8, 9, 10, 11, 12):
         copies[at].wait()
     lows = mm(normed[...], down[...])
@@ -443,11 +492,13 @@
 
         lax.fori_loop(0, width // 256, body, 0)
 
+    phase("proj_kv")
     copies[13].wait()
     project(wk, kbuf, LEN + ctx_n)
     copies[14].wait()
     project(wv, vbuf, LEN + ctx_n)
 
+    phase("ctx_pack")
     lane = lax.broadcasted_iota(jnp.int32, (1, LEN), 1)
     left = lane < HALF
     for p in range(width // LEN):
@@ -473,46 +524,54 @@
 
     lax.fori_loop(1, N_SP, send_ctx, 0)
 
-    copies[15].wait()
-    project(wq, qbuf, LEN)
-    copies[16].wait()
-    project(wb, bbuf, LEN)
-
-    def map_copy(to, carry=None):
-        return remote(map_out.at[to], map_in.at[sp], m_s.at[to], m_r.at[sp], to, tp)
-
-    def chunk(p, carry):
-        at = pl.ds(pl.multiple_of(p * LEN, LEN), LEN)
-        gates = jax.nn.sigmoid(bias[0:1, at] + dbuf[0:LEN, at].astype(f32))
-        rate = jax.nn.sigmoid(bias[1:2, at] + rbuf[0:LEN, at].astype(f32))
-        coming, here, maps = pair_terms(
-            qbuf[:, at].astype(f32),
-            kbuf[0:LEN, at].astype(f32),
-            vbuf[0:LEN, at].astype(f32),
-            -DECAY_TOP * gates,
-            rate,
-        )
-        for direction in (0, 1):
-            for head in (0, 1):
-                map_out[direction * 8 + 2 * p + head] = maps[direction][head].astype(bf16)
-        for direction in (0, 1):
-            for head in (0, 1):
-                to = direction * 8 + 2 * p + head
-
-                @pl.when(to != sp)
-                def _():
-                    map_copy(to).start()
-
-        ahead[p] = coming.astype(bf16)
-        local[p] = here
+    phase("chunks")
+    def place(to):
+        slot = jnp.where(to == sp, N_SP, sp)
+        return slot, jnp.where(to == sp, sibling, tp)
+
+    def chunk(g, carry):
+        inputs, at = [], []
+        for k in range(group):
+            p = g * group + k
+            cols = pl.ds(pl.multiple_of(p * LEN, LEN), LEN)
+            gates = jax.nn.sigmoid(bias[0:1, cols] + dbuf[0:LEN, cols].astype(f32))
+            rate = jax.nn.sigmoid(bias[1:2, cols] + rbuf[0:LEN, cols].astype(f32))
+            inputs.append(
+                (
+                    kbuf[0:LEN, cols].astype(f32),
+                    vbuf[0:LEN, cols].astype(f32),
+                    -DECAY_TOP * gates,
+                    rate,
+                )
+            )
+            at.append(p)
+        found = pairs_terms(inputs)
+        for p, (maps, solved, rights, factors, scale) in zip(at, found):
+            for direction in (0, 1):
+                for head in (0, 1):
+                    map_out[direction * 8 + 2 * p + head] = maps[2 * direction + head].astype(bf16)
+        for p, (maps, solved, rights, factors, scale) in zip(at, found):
+            for direction in (0, 1):
+                for head in (0, 1):
+                    to = direction * 8 + 2 * p + head
+                    slot, over = place(to)
+                    remote(
+                        map_out.at[to], map_in.at[slot], m_s.at[to], m_r.at[slot], to, over
+                    ).start()
+                    solved_buf[p, 2 * direction + head] = solved[2 * direction + head]
+                right_buf[p, direction] = rights[direction]
+                factor_buf[p, direction] = factors[direction]
+            scale_buf[p] = scale
         return carry
 
-    lax.fori_loop(0, width // LEN, chunk, 0)
+    lax.fori_loop(0, width // LEN // group, chunk, 0)
     map_in[sp] = map_out[sp]
 
+    phase("wait_ctx")
     for j in range(1, N_SP):
         frm = (sp + j) % N_SP
         remote(ctx_out.at[0], ctx_in.at[frm], c_s.at[j], c_r.at[frm], sp, tp).wait_recv()
+    phase("ctx_chunks")
     my_bias = head_rows[pl.ds(my_head, 1)]
     per = LEN // ctx_n
     pairs, lows_in = [], []
@@ -521,44 +580,102 @@
         lows_in.append(ctx_in[c * per : (c + 1) * per, :, LEN:].astype(f32).reshape(LEN, LEN))
     for c, found in enumerate(context_terms(pairs, lows_in, my_bias, backward)):
         ctx_maps[c] = found
+    phase("wait_maps")
+    for j in range(1, N_SP + 1):
+        frm = (sp + j) % N_SP if j < N_SP else N_SP
+        remote(map_out.at[0], map_in.at[frm], m_s.at[0], m_r.at[frm], sp, tp).wait_recv()
+    phase("walk")
     count = N_SP // per
     forward = backward == 0
+    order = [jnp.where(forward, i, N_SP - 1 - i) for i in range(N_SP)]
+    steps = [map_in[order[i]].astype(f32) for i in range(N_SP - 1)]
     state = ctx_maps[jnp.where(forward, 0, count - 1)]
     for c in range(1, count):
-        state = advance(state, ctx_maps[jnp.where(forward, c, count - 1 - c)].astype(bf16))
-
+        state = compose(state, ctx_maps[jnp.where(forward, c, count - 1 - c)])
+    two = [compose(steps[2 * i], steps[2 * i + 1]) for i in range(7)]
+    four = [compose(two[2 * i], two[2 * i + 1]) for i in range(3)]
+    eight = compose(four[0], four[1])
     odd = my_head % 2
-    keep = (lane >= HALF) == (odd == 1)
-
-    def walk(i, state):
-        at = jnp.where(forward, i, N_SP - 1 - i)
-        shown = jnp.where(odd == 1, state, pltpu.roll(state, HALF, 1))
-        state_out[at] = jnp.where(keep, shown, 0.0).astype(bf16)
-
-        @pl.when(at != sp)
-        def _():
-            remote(state_out.at[at], states.at[sp], s_s.at[at], s_r.at[sp], at, tp).start()
-            remote(map_out.at[0], map_in.at[at], m_s.at[at], m_r.at[at], sp, tp).wait_recv()
-
-        return advance(state, map_in[at])
-
-    lax.fori_loop(0, N_SP, walk, state)
+    left = lax.broadcasted_iota(jnp.int32, (1, LEN), 1) < HALF
+
+    def show(i, state):
+        to = order[i]
+        state_out[to] = jnp.where(
+            left, pltpu.roll(state[: HALF // 2], HALF, 1), state[HALF // 2 :]
+        ).astype(bf16)
+
+    def launch(i):
+        to = order[i]
+        slot, over = place(to)
+        remote(state_out.at[to], states.at[slot], s_s.at[to], s_r.at[slot], to, over).start()
+
+    held = {0: state}
+    show(0, state)
+    held[8] = compose(state, eight)
+    held[4] = compose(state, four[0])
+    show(8, held[8])
+    show(4, held[4])
+    for i in (0, 8, 4):
+        launch(i)
+    held[12] = compose(held[8], four[2])
+    held[2] = compose(state, two[0])
+    held[6] = compose(held[4], two[2])
+    held[10] = compose(held[8], two[4])
+    held[14] = compose(held[12], two[6])
+    for i in (2, 6, 10, 12, 14):
+        show(i, held[i])
+    for i in (2, 6, 10, 12, 14):
+        launch(i)
+    for i in range(1, N_SP, 2):
+        show(i, compose(held[i - 1], steps[i - 1]))
+    for i in range(1, N_SP, 2):
+        launch(i)
     states[sp] = state_out[sp]
-    for j in range(1, N_SP):
-        frm = (sp + j) % N_SP
+
+    phase("proj_qb")
+    copies[15].wait()
+    project(wq, qbuf, LEN)
+    copies[16].wait()
+    project(wb, bbuf, LEN)
+
+    phase("read_terms")
+
+    def read_terms(p, carry):
+        cols = pl.ds(pl.multiple_of(p * LEN, LEN), LEN)
+        coming, here = pair_reads(
+            qbuf[:, cols].astype(f32),
+            vbuf[0:LEN, cols].astype(f32),
+            [solved_buf[p, i] for i in range(4)],
+            [right_buf[p, i] for i in range(2)],
+            [factor_buf[p, i] for i in range(2)],
+            scale_buf[p],
+        )
+        ahead[p] = coming.astype(bf16)
+        local[p] = here
+        return carry
+
+    lax.fori_loop(0, width // LEN, read_terms, 0)
+
+    phase("wait_states")
+    for j in range(1, N_SP + 1):
+        frm = (sp + j) % N_SP if j < N_SP else N_SP
         remote(state_out.at[0], states.at[frm], s_s.at[0], s_r.at[frm], sp, tp).wait_recv()
 
+    phase("reads")
     copies[17].wait()
     other = lane >= HALF
     for p in range(width // LEN):
         cols = slice(p * LEN, (p + 1) * LEN)
-        both = jnp.concatenate(
-            [
-                states[2 * p : 2 * p + 2].reshape(LEN, LEN),
-                states[8 + 2 * p : 8 + 2 * p + 2].reshape(LEN, LEN),
-            ],
-            axis=0,
-        )
+        blocks_in = []
+        for at in (2 * p, 8 + 2 * p):
+            first, second = states[at].astype(f32), states[at + 1].astype(f32)
+            blocks_in += [
+                jnp.where(left, first, 0.0),
+                jnp.where(left, pltpu.roll(first, HALF, 1), 0.0),
+                jnp.where(left, 0.0, pltpu.roll(second, HALF, 1)),
+                jnp.where(left, 0.0, second),
+            ]
+        both = jnp.concatenate(blocks_in, axis=0).astype(bf16)
         reads = mm(ahead[p], both) + local[p]
 
         def head_mean(x):
@@ -574,9 +691,23 @@
             normal * ggain[0:1, cols] * (gate * jax.nn.sigmoid(gate))
         ).astype(bf16)
 
+    phase("out_proj")
     copies[18].wait()
     n_chunk = arrived.shape[0]
     piece = model // n_chunk
+
+    def pass_on(c):
+        remote(partial.at[c, 0], paired.at[c], o_s.at[c], o_r.at[c], sp, tp).wait_recv()
+        summed[c] = (partial[c, core].astype(f32) + paired[c].astype(f32)).astype(bf16)
+        for j in (2, 1, 3):
+            x = (xx + j) % 4
+            start(
+                remote(
+                    summed.at[c, x], arrived.at[c, xx], g_s.at[c, j], g_r.at[c, xx], sp, 2 * x + core
+                )
+            )
+        arrived[c, xx] = summed[c, xx]
+
     for c in range(n_chunk):
         cols = slice(c * piece, (c + 1) * piece)
         product = mm(mixed[...], wo[:, cols]).astype(bf16)
@@ -589,17 +720,12 @@
                 partial.at[c, 1 - core], paired.at[c], o_s.at[c], o_r.at[c], sp, sibling
             )
         )
-    for c in range(n_chunk):
-        remote(partial.at[c, 0], paired.at[c], o_s.at[c], o_r.at[c], sp, tp).wait_recv()
-        summed[c] = (partial[c, core].astype(f32) + paired[c].astype(f32)).astype(bf16)
-        for j in (2, 1, 3):
-            x = (xx + j) % 4
-            start(
-                remote(
-                    summed.at[c, x], arrived.at[c, xx], g_s.at[c, j], g_r.at[c, xx], sp, 2 * x + core
-                )
-            )
-        arrived[c, xx] = summed[c, xx]
+        if c >= lag:
+            pass_on(c - lag)
+    phase("wait_core")
+    for c in range(n_chunk - lag, n_chunk):
+        pass_on(c)
+    phase("wait_x")
     pieces = []
     for c in range(n_chunk):
         for j in (1, 3, 2):
@@ -611,6 +737,7 @@
         for x in range(1, 4):
             total = total + arrived[c, x].astype(f32)
         pieces.append(total.astype(bf16).astype(f32))
+    phase("final")
     square = sum(jnp.sum(p * p, axis=-1, keepdims=True) for p in pieces)
     inverse = lax.rsqrt(square * (1.0 / model) + NORM_EPS)
     for c in range(n_chunk):
@@ -622,17 +749,22 @@
                 own_rows[:, cols].astype(f32) + mods[j, 4:5] * (value * inverse)
             ).astype(bf16)
 
+    phase("drain")
     for copy in sends:
         copy.wait_send()
 
     def drain_ctx(j, carry):
         remote(ctx_out.at[0], ctx_in.at[0], c_s.at[j], c_r.at[0], sp, tp).wait_send()
-        to = (sp + j) % N_SP
-        remote(map_out.at[0], map_in.at[0], m_s.at[to], m_r.at[0], sp, tp).wait_send()
-        remote(state_out.at[0], states.at[0], s_s.at[to], s_r.at[0], sp, tp).wait_send()
         return carry
 
+    def drain(j, carry):
+        remote(map_out.at[0], map_in.at[0], m_s.at[j], m_r.at[0], sp, tp).wait_send()
+        remote(state_out.at[0], states.at[0], s_s.at[j], s_r.at[0], sp, tp).wait_send()
+        return carry
+
+    lax.fori_loop(0, N_SP, drain, 0)
     lax.fori_loop(1, N_SP, drain_ctx, 0)
+    scopes.close()
 
 
 def on_device(
@@ -681,7 +813,7 @@
         group_gain.reshape(1, -1),
         out_weight,
     )
-    n_chunk = 4
+    n_chunk = 8
     piece = model // n_chunk
     V = pltpu.VMEM
     dma = pltpu.SemaphoreType.DMA
@@ -718,12 +850,16 @@
         V((N_SP, ctx_n, 2 * LEN), bf16),
         V((8, LEN), f32),
         V((N_SP, HALF, LEN), bf16),
-        V((N_SP, HALF, LEN), bf16),
+        V((N_SP + 1, HALF, LEN), bf16),
         V((4, HALF, LEN), f32),
+        V((width // LEN, 4, LEN, LEN), bf16),
+        V((width // LEN, 2, 2 * LEN, LEN), bf16),
+        V((width // LEN, 2, LEN, LEN), f32),
+        V((width // LEN, 1, LEN), f32),
         V((width // LEN, LEN, 2 * LEN), bf16),
         V((width // LEN, LEN, LEN), f32),
-        V((N_SP, HALF, LEN), bf16),
-        V((N_SP, HALF, LEN), bf16),
+        V((N_SP, HALF // 2, LEN), bf16),
+        V((N_SP + 1, HALF // 2, LEN), bf16),
         V((LEN, width), bf16),
         V((n_chunk, 2, 4, own_n, piece), bf16),
         V((n_chunk, 4, own_n, piece), bf16),
@@ -742,9 +878,9 @@
         dma((N_SP,)),
         dma((N_SP,)),
         dma((N_SP,)),
+        dma((N_SP + 1,)),
         dma((N_SP,)),
-        dma((N_SP,)),
-        dma((N_SP,)),
+        dma((N_SP + 1,)),
         dma((n_chunk,)),
         dma((n_chunk,)),
         dma((n_chunk, 4)),

time: 63.3 us -> 55.9 us (0.88)
  Pallas kernels: 61.6 us -> 54.2 us
    pallas_call x1, Pallas kernels: 61.6 us -> 54.2 us  [on_device(): pl.pallas_call(kernel, out_shape=jax.ShapeDtypeStruct((own_n, model), bf1...]
where the time goes in v2:
time: 55.9 us; the launch traced here: 55.8 us
  Pallas kernels  54.2 us (97%)
  local copies, waits for them, and re-layouts  1.57 us (3%)
    pallas_call x1, Pallas kernels, on_device(): pl.pallas_call(kernel, out_shape=jax.ShapeDtypeStruct((own_n, model), bf1...  54.2 us
    unnamed x1, local copies, waits for them, and re-layouts  1.57 us

profile of v2, /device:TPU:1, one launch (start us, length us, event | category | flops | bytes accessed | tf_op | source)
XLA Modules:
  0.0 55.8 jit_solution(10248926950224881602)
XLA Ops:
  0.0 54.2 %shard_map.181 = bf16[16,4096]{1,0:T(8,128)(2,1)} custom-call(bf16[16,4096]{1,0:T(8,128)(2,1)} %latent.1, bf16[32,4096]{1,0:T(8,128)(2,1)} %context.1, f32[1,256]{1,0:T(1,128)} %bitcast.6, f32[1,256]{1,0:T(1,128)} %bitcast.7, bf16[256,512]{1,0:T(8,128)(2,1)} %shift_weight.1, bf16[256,512]{1,0:T(8,128)(2,1)} %scale_weight.1, bf16[256,512]{1,0:T(8,128)(2,1)} %gate_weight.1, ...), custom_call_target="tpu_custom_call" | custom-call | tf_op jit(solution)/shard_map/pallas_call | solution.py:889
  54.2 1.6 %copy.21 = bf16[16,4096]{1,0:T(8,128)(2,1)} copy(bf16[16,4096]{1,0:T(8,128)(2,1)} %shard_map.181) | data formatting | bytes 262144

commit v3 on v2

--- a/solution.py
+++ b/solution.py
@@ -16,11 +16,16 @@
 bf16 = jnp.bfloat16
 f32 = jnp.float32
 LEN = 128
-group = 2
 lag = 5
 N_SP = 16
 N_TP = 8
 HALF = 64
+FAR_FIRST = (
+    (2, 2), (2, 1), (2, 3), (1, 2), (3, 2), (1, 1), (3, 3), (1, 3), (3, 1),
+    (2, 0), (0, 2), (1, 0), (3, 0), (0, 1), (0, 3),
+)
+EVEN_FIRST = ((2, 2), (1, 2), (3, 2), (2, 0), (0, 2), (1, 0), (3, 0), (0, 0))
+ODD_FIRST = ((2, 1), (2, 3), (1, 1), (3, 3), (1, 3), (3, 1), (0, 1), (0, 3))
 
 
 def mm(a, b):
@@ -271,6 +276,10 @@
     zpart,
     zbuf,
     mods,
+    gpart,
+    gbuf,
+    gsum,
+    gmods,
     normed,
     low,
     kbuf,
@@ -318,12 +327,20 @@
     o_r,
     g_s,
     g_r,
+    gs_s,
+    gs_r,
+    gt_s,
+    gt_r,
 ):
     sp = lax.axis_index("sp")
     tp = lax.axis_index("tp")
     zz, yy = sp // 4, sp % 4
     xx, core = tp // 2, tp % 2
     sibling = 2 * xx + (1 - core)
+
+    def at_offset(dz, dy):
+        return ((zz + dz) % 4) * 4 + (yy + dy) % 4
+
     width = wq.shape[1]
     model = normed.shape[1]
     blocks = model // width
@@ -339,20 +356,13 @@
     phase("greet")
     barrier = pltpu.get_barrier_semaphore()
 
-    def greet_sp(j, carry):
-        pl.semaphore_signal(
-            barrier, inc=1, device_id=((sp + j) % N_SP, tp), device_id_type=MESH
-        )
-        return carry
-
-    def greet_tp(j, carry):
+    for j in (2, 1, 3):
+        for to in (zz * 4 + (yy + j) % 4, ((zz + j) % 4) * 4 + yy):
+            pl.semaphore_signal(barrier, inc=1, device_id=(to, tp), device_id_type=MESH)
+    for j in range(1, N_TP):
         pl.semaphore_signal(
             barrier, inc=1, device_id=(sp, (tp + j) % N_TP), device_id_type=MESH
         )
-        return carry
-
-    lax.fori_loop(1, N_SP, greet_sp, 0)
-    lax.fori_loop(1, N_TP, greet_tp, 0)
 
     def fetch(at, src, dst):
         return pltpu.make_async_copy(src, dst, load.at[at])
@@ -363,7 +373,6 @@
         fetch(2, shift_weight, mod_w.at[0]),
         fetch(3, scale_weight, mod_w.at[1]),
         fetch(4, gate_weight, mod_w.at[2]),
-        fetch(5, latent, own_rows),
         fetch(6, context, ctx_rows),
         fetch(7, norm_gain, gain),
         fetch(8, decay_down, down.at[:, 0:LEN]),
@@ -378,8 +387,25 @@
         fetch(17, group_gain, ggain),
         fetch(18, out_weight, wo),
     ]
-    for copy in copies:
+    copies.insert(5, fetch(5, latent, own_rows))
+    copies[5].start()
+    for copy in copies[:5] + copies[6:]:
         copy.start()
+
+    phase("barrier")
+    copies[5].wait()
+    pl.semaphore_wait(barrier, 6 + N_TP - 1)
+    sends = []
+
+    def start(copy):
+        copy.start()
+        sends.append(copy)
+
+    for j in (2, 1, 3):
+        to = 2 * ((xx + j) % 4) + core
+        start(remote(own_rows, rows.at[tp], l_s.at[j], l_r.at[tp], sp, to))
+    start(remote(own_rows, rows.at[tp], l_s.at[0], l_r.at[tp], sp, sibling))
+    rows[tp] = own_rows[...]
 
     phase("wait_mod_w")
     for at in (0, 1, 2, 3, 4):
@@ -389,37 +415,31 @@
     conditions = (rows_c * jax.nn.sigmoid(rows_c)).astype(bf16)
     conditions = jnp.concatenate([conditions, jnp.zeros((14, rows_c.shape[1]), bf16)], axis=0)
     shares = [mm(conditions, mod_w[at]) for at in range(3)]
+    halves = (slice(0, width // 2), slice(width // 2, width))
     part[...] = jnp.concatenate(
-        [shares[0][0:2], shares[1][0:2], shares[2][0:1], jnp.zeros((3, width), f32)], axis=0
+        [share[0:2, half] for half in halves for share in shares[:2]], axis=0
+    )
+    gpart[...] = jnp.concatenate(
+        [shares[2][0:1, k * LEN : (k + 1) * LEN] for k in range(width // LEN)]
+        + [jnp.zeros((8 - width // LEN, LEN), f32)],
+        axis=0,
     )
     ybuf[yy] = part[...]
-    phase("barrier")
-    pl.semaphore_wait(barrier, N_SP - 1 + N_TP - 1)
-
+    gbuf[0, yy] = gpart[...]
     phase("send_y")
-    sends = []
-
-    def start(copy):
-        copy.start()
-        sends.append(copy)
-
+    for j in (2, 1, 3):
+        to = zz * 4 + (yy + j) % 4
+        start(remote(part, ybuf.at[yy], y_s.at[j], y_r.at[yy], to, tp))
     for j in (1, 2, 3):
         to = zz * 4 + (yy + j) % 4
-        start(remote(part, ybuf.at[yy], y_s.at[j], y_r.at[yy], to, tp))
-    copies[5].wait()
-    for j in (2, 1, 3):
-        to = 2 * ((xx + j) % 4) + core
-        start(remote(own_rows, rows.at[tp], l_s.at[j], l_r.at[tp], sp, to))
-    start(remote(own_rows, rows.at[tp], l_s.at[0], l_r.at[tp], sp, sibling))
-    rows[tp] = own_rows[...]
-
+        start(remote(gpart, gbuf.at[0, yy], gs_s.at[0, j], gs_r.at[0, yy], to, tp))
     phase("wait_y")
     for j in (1, 2, 3):
         frm = (yy + j) % 4
         remote(part, ybuf.at[frm], y_s.at[j], y_r.at[frm], sp, tp).wait_recv()
     zpart[...] = ybuf[0] + ybuf[1] + ybuf[2] + ybuf[3]
     zbuf[zz] = zpart[...]
-    for j in (1, 2, 3):
+    for j in (2, 1, 3):
         to = ((zz + j) % 4) * 4 + yy
         start(remote(zpart, zbuf.at[zz], z_s.at[j], z_r.at[zz], to, tp))
 
@@ -434,8 +454,8 @@
         remote(zpart, zbuf.at[frm], z_s.at[j], z_r.at[frm], sp, tp).wait_recv()
     part2 = zbuf[0] + zbuf[1] + zbuf[2] + zbuf[3]
     mods[tp] = part2
-    for j in range(1, N_TP):
-        to = (tp + j) % N_TP
+    for j in (4, 5, 2, 3, 6, 7, 1):
+        to = 2 * ((xx + j // 2) % 4) + (core + j) % 2
         start(remote(mods.at[tp], mods.at[tp], t_s.at[j], t_r.at[tp], sp, to))
 
     phase("latent_x")
@@ -460,9 +480,9 @@
         remote(part, mods.at[frm], t_s.at[j], t_r.at[frm], sp, tp).wait_recv()
 
     phase("normalize")
-    for j in range(blocks):
-        cols = slice(j * width, (j + 1) * width)
-        vectors = mods[j]
+    for j in range(2 * blocks):
+        cols = slice(j * width // 2, (j + 1) * width // 2)
+        vectors = mods[j // 2, 4 * (j % 2) : 4 * (j % 2) + 4]
         factor = gain[0:1, cols] * (1.0 + vectors[2:3])
         shift = vectors[0:1]
         for i in range(N_TP):
@@ -474,6 +494,15 @@
         normed[LEN : LEN + ctx_n, cols] = (
             ctx_rows[:, cols].astype(f32) * ctx_scale * factor + shift
         ).astype(bf16)
+
+    for j in (1, 2, 3):
+        frm = (yy + j) % 4
+        remote(gpart, gbuf.at[0, frm], gs_s.at[0, j], gs_r.at[0, frm], sp, tp).wait_recv()
+    gsum[0] = gbuf[0, 0] + gbuf[0, 1] + gbuf[0, 2] + gbuf[0, 3]
+    gbuf[1, zz] = gsum[0]
+    for j in (1, 2, 3):
+        to = ((zz + j) % 4) * 4 + yy
+        start(remote(gsum.at[0], gbuf.at[1, zz], gs_s.at[1, j], gs_r.at[1, zz], to, tp))
 
     phase("lows")
     for at in (8, 9, 10, 11, 12):
@@ -517,23 +546,24 @@
     backward = sp // 8
     ctx_in[sp] = ctx_out[my_head]
 
-    def send_ctx(j, carry):
-        to = (sp + j) % N_SP
-        remote(ctx_out.at[to % 8], ctx_in.at[sp], c_s.at[j], c_r.at[sp], to, tp).start()
-        return carry
-
-    lax.fori_loop(1, N_SP, send_ctx, 0)
+    for dz, dy in FAR_FIRST:
+        to = at_offset(dz, dy)
+        start(
+            remote(
+                ctx_out.at[to % 8], ctx_in.at[sp], c_s.at[4 * dz + dy], c_r.at[sp], to, tp
+            )
+        )
 
     phase("chunks")
     def place(to):
         slot = jnp.where(to == sp, N_SP, sp)
         return slot, jnp.where(to == sp, sibling, tp)
 
-    def chunk(g, carry):
+    def chunk():
         inputs, at = [], []
-        for k in range(group):
-            p = g * group + k
-            cols = pl.ds(pl.multiple_of(p * LEN, LEN), LEN)
+        for k in range(width // LEN):
+            p = k
+            cols = slice(p * LEN, (p + 1) * LEN)
             gates = jax.nn.sigmoid(bias[0:1, cols] + dbuf[0:LEN, cols].astype(f32))
             rate = jax.nn.sigmoid(bias[1:2, cols] + rbuf[0:LEN, cols].astype(f32))
             inputs.append(
@@ -550,22 +580,27 @@
             for direction in (0, 1):
                 for head in (0, 1):
                     map_out[direction * 8 + 2 * p + head] = maps[2 * direction + head].astype(bf16)
+        for dz, dy in FAR_FIRST:
+            to = at_offset(dz, dy)
+            start(remote(map_out.at[to], map_in.at[sp], m_s.at[to], m_r.at[sp], to, tp))
         for p, (maps, solved, rights, factors, scale) in zip(at, found):
             for direction in (0, 1):
                 for head in (0, 1):
-                    to = direction * 8 + 2 * p + head
-                    slot, over = place(to)
-                    remote(
-                        map_out.at[to], map_in.at[slot], m_s.at[to], m_r.at[slot], to, over
-                    ).start()
                     solved_buf[p, 2 * direction + head] = solved[2 * direction + head]
                 right_buf[p, direction] = rights[direction]
                 factor_buf[p, direction] = factors[direction]
             scale_buf[p] = scale
-        return carry
-
-    lax.fori_loop(0, width // LEN // group, chunk, 0)
+
+    chunk()
     map_in[sp] = map_out[sp]
+
+    for j in (1, 2, 3):
+        frm = (zz + j) % 4
+        remote(gpart, gbuf.at[1, frm], gs_s.at[1, j], gs_r.at[1, frm], sp, tp).wait_recv()
+    gmods[tp] = gbuf[1, 0] + gbuf[1, 1] + gbuf[1, 2] + gbuf[1, 3]
+    for j in range(1, N_TP):
+        to = (tp + j) % N_TP
+        start(remote(gmods.at[tp], gmods.at[tp], gt_s.at[j], gt_r.at[tp], sp, to))
 
     phase("wait_ctx")
     for j in range(1, N_SP):
@@ -580,9 +615,15 @@
         lows_in.append(ctx_in[c * per : (c + 1) * per, :, LEN:].astype(f32).reshape(LEN, LEN))
     for c, found in enumerate(context_terms(pairs, lows_in, my_bias, backward)):
         ctx_maps[c] = found
+    phase("proj_b")
+    copies[16].wait()
+    project(wb, bbuf, LEN)
     phase("wait_maps")
-    for j in range(1, N_SP + 1):
-        frm = (sp + j) % N_SP if j < N_SP else N_SP
+    for copy in sends:
+        copy.wait_send()
+    drained = len(sends)
+    for j in range(1, N_SP):
+        frm = (sp + j) % N_SP
         remote(map_out.at[0], map_in.at[frm], m_s.at[0], m_r.at[frm], sp, tp).wait_recv()
     phase("walk")
     count = N_SP // per
@@ -604,8 +645,7 @@
             left, pltpu.roll(state[: HALF // 2], HALF, 1), state[HALF // 2 :]
         ).astype(bf16)
 
-    def launch(i):
-        to = order[i]
+    def launch(to):
         slot, over = place(to)
         remote(state_out.at[to], states.at[slot], s_s.at[to], s_r.at[slot], to, over).start()
 
@@ -616,7 +656,7 @@
     show(8, held[8])
     show(4, held[4])
     for i in (0, 8, 4):
-        launch(i)
+        launch(order[i])
     held[12] = compose(held[8], four[2])
     held[2] = compose(state, two[0])
     held[6] = compose(held[4], two[2])
@@ -625,19 +665,17 @@
     for i in (2, 6, 10, 12, 14):
         show(i, held[i])
     for i in (2, 6, 10, 12, 14):
-        launch(i)
+        launch(order[i])
     for i in range(1, N_SP, 2):
         show(i, compose(held[i - 1], steps[i - 1]))
-    for i in range(1, N_SP, 2):
-        launch(i)
+    even = (yy % 2 == 0) == (backward == 1)
+    for one, other in zip(EVEN_FIRST, ODD_FIRST):
+        launch(jnp.where(even, at_offset(*one), at_offset(*other)))
     states[sp] = state_out[sp]
 
     phase("proj_qb")
     copies[15].wait()
     project(wq, qbuf, LEN)
-    copies[16].wait()
-    project(wb, bbuf, LEN)
-
     phase("read_terms")
 
     def read_terms(p, carry):
@@ -662,6 +700,9 @@
         remote(state_out.at[0], states.at[frm], s_s.at[0], s_r.at[frm], sp, tp).wait_recv()
 
     phase("reads")
+    for j in range(1, N_TP):
+        frm = (tp + j) % N_TP
+        remote(gpart, gmods.at[frm], gt_s.at[j], gt_r.at[frm], sp, tp).wait_recv()
     copies[17].wait()
     other = lane >= HALF
     for p in range(width // LEN):
@@ -696,17 +737,27 @@
     n_chunk = arrived.shape[0]
     piece = model // n_chunk
 
+    def chip_sum(c, x):
+        return partial[c, core, x].astype(f32) + paired[c, x].astype(f32)
+
+    def send_x(c, j):
+        x = (xx + j) % 4
+        start(
+            remote(
+                summed.at[c, j - 1], arrived.at[c, j - 1], g_s.at[c, j - 1], g_r.at[c, j - 1], sp,
+                2 * x + core,
+            )
+        )
+
     def pass_on(c):
         remote(partial.at[c, 0], paired.at[c], o_s.at[c], o_r.at[c], sp, tp).wait_recv()
-        summed[c] = (partial[c, core].astype(f32) + paired[c].astype(f32)).astype(bf16)
         for j in (2, 1, 3):
-            x = (xx + j) % 4
-            start(
-                remote(
-                    summed.at[c, x], arrived.at[c, xx], g_s.at[c, j], g_r.at[c, xx], sp, 2 * x + core
-                )
-            )
-        arrived[c, xx] = summed[c, xx]
+            summed[c, j - 1] = chip_sum(c, (xx + j) % 4).astype(bf16)
+        send_x(c, 2)
+        if c % 2 == 1:
+            for at in (c - 1, c):
+                send_x(at, 1)
+                send_x(at, 3)
 
     for c in range(n_chunk):
         cols = slice(c * piece, (c + 1) * piece)
@@ -728,42 +779,33 @@
     phase("wait_x")
     pieces = []
     for c in range(n_chunk):
-        for j in (1, 3, 2):
-            x = (xx + j) % 4
+        for k in (0, 2, 1):
             remote(
-                summed.at[c, 0], arrived.at[c, x], g_s.at[c, j], g_r.at[c, x], sp, tp
+                summed.at[c, 0], arrived.at[c, k], g_s.at[c, k], g_r.at[c, k], sp, tp
             ).wait_recv()
-        total = arrived[c, 0].astype(f32)
-        for x in range(1, 4):
-            total = total + arrived[c, x].astype(f32)
+        total = chip_sum(c, xx)
+        for k in range(3):
+            total = total + arrived[c, k].astype(f32)
         pieces.append(total.astype(bf16).astype(f32))
     phase("final")
     square = sum(jnp.sum(p * p, axis=-1, keepdims=True) for p in pieces)
     inverse = lax.rsqrt(square * (1.0 / model) + NORM_EPS)
     for c in range(n_chunk):
-        for s in range(piece // width):
-            j = c * (piece // width) + s
-            cols = slice(j * width, (j + 1) * width)
-            value = pieces[c][:, s * width : (s + 1) * width]
-            out[:, cols] = (
-                own_rows[:, cols].astype(f32) + mods[j, 4:5] * (value * inverse)
-            ).astype(bf16)
+        for k in range(piece // LEN):
+            lo = c * piece + k * LEN
+            cols = slice(lo, lo + LEN)
+            lane_block = lo // LEN
+            per_tp = width // LEN
+            gate = gmods[lane_block // per_tp, lane_block % per_tp : lane_block % per_tp + 1]
+            value = pieces[c][:, k * LEN : (k + 1) * LEN]
+            out[:, cols] = (own_rows[:, cols].astype(f32) + gate * (value * inverse)).astype(bf16)
 
     phase("drain")
-    for copy in sends:
+    for copy in sends[drained:]:
         copy.wait_send()
 
-    def drain_ctx(j, carry):
-        remote(ctx_out.at[0], ctx_in.at[0], c_s.at[j], c_r.at[0], sp, tp).wait_send()
-        return carry
-
-    def drain(j, carry):
-        remote(map_out.at[0], map_in.at[0], m_s.at[j], m_r.at[0], sp, tp).wait_send()
+    for j in range(N_SP):
         remote(state_out.at[0], states.at[0], s_s.at[j], s_r.at[0], sp, tp).wait_send()
-        return carry
-
-    lax.fori_loop(0, N_SP, drain, 0)
-    lax.fori_loop(1, N_SP, drain_ctx, 0)
     scopes.close()
 
 
@@ -833,11 +875,15 @@
         V((model, width), bf16),
         V((1, width), f32),
         V((width, model), bf16),
-        V((8, width), f32),
-        V((4, 8, width), f32),
-        V((8, width), f32),
-        V((4, 8, width), f32),
-        V((N_TP, 8, width), f32),
+        V((8, width // 2), f32),
+        V((4, 8, width // 2), f32),
+        V((8, width // 2), f32),
+        V((4, 8, width // 2), f32),
+        V((N_TP, 8, width // 2), f32),
+        V((8, LEN), f32),
+        V((2, 4, 8, LEN), f32),
+        V((1, 8, LEN), f32),
+        V((N_TP, 8, LEN), f32),
         V((LEN + ctx_n, model), bf16),
         V((LEN + ctx_n, 2 * LEN), bf16),
         V((LEN + ctx_n, width), bf16),
@@ -863,8 +909,8 @@
         V((LEN, width), bf16),
         V((n_chunk, 2, 4, own_n, piece), bf16),
         V((n_chunk, 4, own_n, piece), bf16),
-        V((n_chunk, 4, own_n, piece), bf16),
-        V((n_chunk, 4, own_n, piece), bf16),
+        V((n_chunk, 3, own_n, piece), bf16),
+        V((n_chunk, 3, own_n, piece), bf16),
         dma((19,)),
         dma((4,)),
         dma((4,)),
@@ -883,8 +929,12 @@
         dma((N_SP + 1,)),
         dma((n_chunk,)),
         dma((n_chunk,)),
-        dma((n_chunk, 4)),
-        dma((n_chunk, 4)),
+        dma((n_chunk, 3)),
+        dma((n_chunk, 3)),
+        dma((2, 4)),
+        dma((2, 4)),
+        dma((N_TP,)),
+        dma((N_TP,)),
     ]
     return pl.pallas_call(
         kernel,

time: 55.9 us -> 52.9 us (0.946)
  Pallas kernels: 54.2 us -> 51.2 us
    pallas_call x1, Pallas kernels: 54.2 us -> 51.2 us  [on_device(): pl.pallas_call(kernel, out_shape=jax.ShapeDtypeStruct((own_n, model), bf1...]
where the time goes in v3:
time: 52.9 us; the launch traced here: 52.8 us
  Pallas kernels  51.2 us (97%)
  local copies, waits for them, and re-layouts  1.57 us (3%)
    pallas_call x1, Pallas kernels, on_device(): pl.pallas_call(kernel, out_shape=jax.ShapeDtypeStruct((own_n, model), bf1...  51.2 us
    unnamed x1, local copies, waits for them, and re-layouts  1.57 us

profile of v3, /device:TPU:1, one launch (start us, length us, event | category | flops | bytes accessed | tf_op | source)
XLA Modules:
  0.0 52.8 jit_solution(6659142826805885618)
XLA Ops:
  0.0 51.2 %shard_map.181 = bf16[16,4096]{1,0:T(8,128)(2,1)} custom-call(bf16[16,4096]{1,0:T(8,128)(2,1)} %latent.1, bf16[32,4096]{1,0:T(8,128)(2,1)} %context.1, f32[1,256]{1,0:T(1,128)} %bitcast.6, f32[1,256]{1,0:T(1,128)} %bitcast.7, bf16[256,512]{1,0:T(8,128)(2,1)} %shift_weight.1, bf16[256,512]{1,0:T(8,128)(2,1)} %scale_weight.1, bf16[256,512]{1,0:T(8,128)(2,1)} %gate_weight.1, ...), custom_call_target="tpu_custom_call" | custom-call | tf_op jit(solution)/shard_map/pallas_call | solution.py:939
  51.2 1.6 %copy.21 = bf16[16,4096]{1,0:T(8,128)(2,1)} copy(bf16[16,4096]{1,0:T(8,128)(2,1)} %shard_map.181) | data formatting | bytes 262144

commit v4 on v3

--- a/solution.py
+++ b/solution.py
@@ -73,6 +73,49 @@
     return [y + mm(d, p.astype(bf16)) for y, d, p in zip(first, low, part)]
 
 
+def solve_both(couplings, sides, row, col):
+    cross = row ^ col
+    lower, upper = row >= col, row <= col
+    eye = jnp.where(row == col, 1.0, 0.0)
+    held = [eye + jnp.where(cross == 1, a, 0.0) for a in couplings]
+    size = 2
+    while size < LEN // 2:
+        late = (row & size) != 0
+        level = (cross >= size) & (cross < 2 * size)
+        inner = (late & upper) | (~late & lower)
+        outer = (late & lower) | (~late & upper)
+        part = [
+            mm(jnp.where(level, a, 0.0).astype(bf16), jnp.where(inner, h, 0.0).astype(bf16))
+            for a, h in zip(couplings, held)
+        ]
+        held = [
+            h + mm(jnp.where(outer, h, 0.0).astype(bf16), p.astype(bf16))
+            for h, p in zip(held, part)
+        ]
+        size *= 2
+    late = (row & size) != 0
+    level = (cross >= size) & (cross < 2 * size)
+    outer = (late & lower) | (~late & upper)
+    first = [
+        (
+            mm(jnp.where(lower, h, 0.0).astype(bf16), f.astype(bf16)),
+            mm(jnp.where(upper, h, 0.0).astype(bf16), b.astype(bf16)),
+        )
+        for h, (f, b) in zip(held, sides)
+    ]
+    part = [
+        mm(jnp.where(level, a, 0.0).astype(bf16), jnp.where(late, b, f).astype(bf16))
+        for a, (f, b) in zip(couplings, first)
+    ]
+    last = [
+        mm(jnp.where(outer, h, 0.0).astype(bf16), p.astype(bf16)) for h, p in zip(held, part)
+    ]
+    return [
+        (f + jnp.where(late, u, 0.0), b + jnp.where(late, 0.0, u))
+        for (f, b), u in zip(first, last)
+    ]
+
+
 def head_mask(head):
     lane = lax.broadcasted_iota(jnp.int32, (1, LEN), 1)
     return (lane >= HALF) if head else (lane < HALF)
@@ -113,7 +156,7 @@
     crossed_values = pltpu.roll(values, HALF, 1)
     fed_by = crossed_values.astype(bf16)
     own = [head_mask(0), head_mask(1)]
-    units, rights, factors = [], [], []
+    couplings, sides, rights, factors, transposes = [], [], [], [], []
     for direction in (0, 1):
         left, right = (before, after) if direction == 0 else (after, before)
         er = erase * left
@@ -121,37 +164,45 @@
         right_both = jnp.concatenate([wr, kr], axis=0).astype(bf16)
         rights.append(right_both)
         factors.append(left * step)
-        transposed = jnp.concatenate(
-            [jnp.transpose(wr * scale), jnp.transpose(kr * scale)], axis=1
-        ).astype(bf16)
+        transposes.append(
+            jnp.concatenate(
+                [jnp.transpose(wr * scale), jnp.transpose(kr * scale)], axis=1
+            ).astype(bf16)
+        )
         left_both = jnp.concatenate([jnp.where(mask, er, 0.0) for mask in own], axis=0)
         grams = mm_nt(left_both.astype(bf16), right_both)
         strict = (row > col) if direction == 0 else (row < col)
         for head in (0, 1):
             rows = slice(head * LEN, (head + 1) * LEN)
-            coupling = jnp.where(strict, grams[rows, :LEN], 0.0)
+            couplings.append(grams[rows, :LEN])
             feeding = jnp.where(strict, grams[rows, LEN:], 0.0).astype(bf16)
-            side = jnp.where(own[head], er, mm(feeding, fed_by))
-            units.append((coupling, side, transposed, head))
-    return units, rights, factors, crossed_values, scale, total
+            sides.append(jnp.where(own[head], er, mm(feeding, fed_by)))
+    couplings = [jnp.where(row > col, couplings[h], couplings[2 + h]) for h in (0, 1)]
+    sides = [(sides[h], sides[2 + h]) for h in (0, 1)]
+    return couplings, sides, transposes, rights, factors, crossed_values, scale, total
 
 
 def pairs_terms(inputs):
     row, col = rows_cols()
     setups = [pair_setup(*given, row, col) for given in inputs]
-    flat = [unit for setup in setups for unit in setup[0]]
-    answers = solve([u[0] for u in flat], [u[1] for u in flat], row ^ col)
-    results, at = [], 0
-    for units, rights, factors, crossed_values, scale, total in setups:
+    answers = solve_both(
+        [a for setup in setups for a in setup[0]],
+        [side for setup in setups for side in setup[1]],
+        row,
+        col,
+    )
+    results = []
+    for k, setup in enumerate(setups):
+        _, _, transposes, rights, factors, crossed_values, scale, total = setup
         maps, solved = [], []
-        for _, _, transposed, head in units:
-            mine = head_mask(head)
-            answer = answers[at]
-            at += 1
-            rows = jnp.where(mine, answer * scale, answer).astype(bf16)
-            crossed = jnp.where(mine, 0.0, crossed_values).astype(bf16)
-            maps.append(state_map(transposed, rows, crossed, total, head))
-            solved.append(rows)
+        for direction in (0, 1):
+            for head in (0, 1):
+                mine = head_mask(head)
+                answer = answers[2 * k + head][direction]
+                rows = jnp.where(mine, answer * scale, answer).astype(bf16)
+                crossed = jnp.where(mine, 0.0, crossed_values).astype(bf16)
+                maps.append(state_map(transposes[direction], rows, crossed, total, head))
+                solved.append(rows)
         results.append((maps, solved, rights, factors, scale))
     return results
 
@@ -256,6 +307,7 @@
     group_gain,
     out_weight,
     out,
+    result,
     rows,
     own_rows,
     ctx_rows,
@@ -798,14 +850,17 @@
             per_tp = width // LEN
             gate = gmods[lane_block // per_tp, lane_block % per_tp : lane_block % per_tp + 1]
             value = pieces[c][:, k * LEN : (k + 1) * LEN]
-            out[:, cols] = (own_rows[:, cols].astype(f32) + gate * (value * inverse)).astype(bf16)
+            result[:, cols] = (own_rows[:, cols].astype(f32) + gate * (value * inverse)).astype(bf16)
 
     phase("drain")
+    put = pltpu.make_async_copy(result, out, load.at[0])
+    put.start()
     for copy in sends[drained:]:
         copy.wait_send()
 
     for j in range(N_SP):
         remote(state_out.at[0], states.at[0], s_s.at[j], s_r.at[0], sp, tp).wait_send()
+    put.wait()
     scopes.close()
 
 
@@ -860,6 +915,7 @@
     V = pltpu.VMEM
     dma = pltpu.SemaphoreType.DMA
     scratch = [
+        V((own_n, model), bf16),
         V((N_TP, own_n, model), bf16),
         V((own_n, model), bf16),
         V((ctx_n, model), bf16),
@@ -939,13 +995,13 @@
     return pl.pallas_call(
         kernel,
         out_shape=jax.ShapeDtypeStruct((own_n, model), bf16),
-        in_specs=[pl.BlockSpec(memory_space=pl.ANY)] * len(args),
-        out_specs=pl.BlockSpec(memory_space=pltpu.VMEM),
+        in_specs=[pl.BlockSpec(memory_space=pltpu.HBM)] * len(args),
+        out_specs=pl.BlockSpec(memory_space=pl.ANY),
         scratch_shapes=scratch,
         compiler_params=pltpu.CompilerParams(
-            collective_id=0, has_side_effects=True, vmem_limit_bytes=60 * 1024 * 1024
+            collective_id=0, has_side_effects=True, vmem_limit_bytes=44 * 1024 * 1024
         ),
-    )(*args)
+    )(*(pltpu.with_memory_space_constraint(a, pltpu.HBM) for a in args))
 
 
 def solution(mesh):

time: 52.9 us -> 51.6 us (0.975)
  local copies, waits for them, and re-layouts: 1.57 us -> 0.66 us
    unnamed x1, local copies, waits for them, and re-layouts: 1.57 us -> 0.66 us
where the time goes in v4:
time: 51.6 us; the launch traced here: 51.5 us
  Pallas kernels  50.8 us (98%)
  local copies, waits for them, and re-layouts  0.66 us (1%)
    pallas_call x1, Pallas kernels, on_device(): pl.pallas_call(kernel, out_shape=jax.ShapeDtypeStruct((own_n, model), bf1...  50.8 us

profile of v4, /device:TPU:1, one launch (start us, length us, event | category | flops | bytes accessed | tf_op | source)
XLA Modules:
  0.0 51.5 jit_solution(1833150885021209195)
XLA Ops:
  0.0 50.8 %shard_map.181 = bf16[16,4096]{1,0:T(8,128)(2,1)S(1)} custom-call(bf16[16,4096]{1,0:T(8,128)(2,1)} %latent.1, bf16[32,4096]{1,0:T(8,128)(2,1)} %context.1, f32[1,256]{1,0:T(1,128)} %bitcast.6, f32[1,256]{1,0:T(1,128)} %bitcast.7, bf16[256,512]{1,0:T(8,128)(2,1)} %shift_weight.1, bf16[256,512]{1,0:T(8,128)(2,1)} %scale_weight.1, ...), custom_call_target="tpu_custom_call" | custom-call | tf_op jit(solution)/shard_map/pallas_call | solution.py:995
  50.8 0.7 %copy.21 = bf16[16,4096]{1,0:T(8,128)(2,1)} copy(bf16[16,4096]{1,0:T(8,128)(2,1)S(1)} %shard_map.181) | data formatting | bytes 262144

commit v5 on v4

--- a/solution.py
+++ b/solution.py
@@ -24,8 +24,6 @@
     (2, 2), (2, 1), (2, 3), (1, 2), (3, 2), (1, 1), (3, 3), (1, 3), (3, 1),
     (2, 0), (0, 2), (1, 0), (3, 0), (0, 1), (0, 3),
 )
-EVEN_FIRST = ((2, 2), (1, 2), (3, 2), (2, 0), (0, 2), (1, 0), (3, 0), (0, 0))
-ODD_FIRST = ((2, 1), (2, 3), (1, 1), (3, 3), (1, 3), (3, 1), (0, 1), (0, 3))
 
 
 def mm(a, b):
@@ -142,68 +140,64 @@
     return pltpu.roll(out, HALF, 1) if head else out
 
 
-def pair_setup(keys, values, log_decay, rate, row, col):
-    cum = cumulative(log_decay, row, col)
-    total = cum[LEN - 1 : LEN]
-    half = 0.5 * total
-    scale = jnp.exp(half)
-    unit = pair_unit(keys)
-    erase = -unit
-    write = unit * rate
-    before = jnp.exp(cum - log_decay - half)
-    after = jnp.exp(half - cum)
-    step = jnp.exp(log_decay)
-    crossed_values = pltpu.roll(values, HALF, 1)
-    fed_by = crossed_values.astype(bf16)
+def pairs_terms(inputs, keep):
+    row, col = rows_cols()
     own = [head_mask(0), head_mask(1)]
-    couplings, sides, rights, factors, transposes = [], [], [], [], []
-    for direction in (0, 1):
-        left, right = (before, after) if direction == 0 else (after, before)
-        er = erase * left
-        wr, kr = write * right, keys * right
-        right_both = jnp.concatenate([wr, kr], axis=0).astype(bf16)
-        rights.append(right_both)
-        factors.append(left * step)
-        transposes.append(
-            jnp.concatenate(
-                [jnp.transpose(wr * scale), jnp.transpose(kr * scale)], axis=1
-            ).astype(bf16)
-        )
-        left_both = jnp.concatenate([jnp.where(mask, er, 0.0) for mask in own], axis=0)
-        grams = mm_nt(left_both.astype(bf16), right_both)
-        strict = (row > col) if direction == 0 else (row < col)
+    cums = [cumulative(log_decay, row, col) for _, _, log_decay, _ in inputs]
+    stages = []
+    for k, ((keys, values, log_decay, rate), cum) in enumerate(zip(inputs, cums)):
+        total = cum[LEN - 1 : LEN]
+        half = 0.5 * total
+        scale = jnp.exp(half)
+        unit = pair_unit(keys)
+        erase = -unit
+        write = unit * rate
+        before = jnp.exp(cum - log_decay - half)
+        after = jnp.exp(half - cum)
+        step = jnp.exp(log_decay)
+        erases, grams, transposes, rights, factors = [], [], [], [], []
+        for direction in (0, 1):
+            left, right = (before, after) if direction == 0 else (after, before)
+            er = erase * left
+            wr, kr = write * right, keys * right
+            right_both = jnp.concatenate([wr, kr], axis=0).astype(bf16)
+            left_both = jnp.concatenate([jnp.where(mask, er, 0.0) for mask in own], axis=0)
+            grams.append(mm_nt(left_both.astype(bf16), right_both))
+            erases.append(er)
+            rights.append(right_both)
+            factors.append(left * step)
+            transposes.append(
+                jnp.concatenate(
+                    [jnp.transpose(wr * scale), jnp.transpose(kr * scale)], axis=1
+                ).astype(bf16)
+            )
+        keep(k, rights, factors, scale)
+        stages.append((erases, grams, transposes, pltpu.roll(values, HALF, 1), scale, total))
+    couplings, sides = [], []
+    for erases, grams, _, crossed_values, _, _ in stages:
+        fed_by = crossed_values.astype(bf16)
         for head in (0, 1):
             rows = slice(head * LEN, (head + 1) * LEN)
-            couplings.append(grams[rows, :LEN])
-            feeding = jnp.where(strict, grams[rows, LEN:], 0.0).astype(bf16)
-            sides.append(jnp.where(own[head], er, mm(feeding, fed_by)))
-    couplings = [jnp.where(row > col, couplings[h], couplings[2 + h]) for h in (0, 1)]
-    sides = [(sides[h], sides[2 + h]) for h in (0, 1)]
-    return couplings, sides, transposes, rights, factors, crossed_values, scale, total
-
-
-def pairs_terms(inputs):
-    row, col = rows_cols()
-    setups = [pair_setup(*given, row, col) for given in inputs]
-    answers = solve_both(
-        [a for setup in setups for a in setup[0]],
-        [side for setup in setups for side in setup[1]],
-        row,
-        col,
-    )
+            couplings.append(jnp.where(row > col, grams[0][rows, :LEN], grams[1][rows, :LEN]))
+            pair = []
+            for direction in (0, 1):
+                strict = (row > col) if direction == 0 else (row < col)
+                feeding = jnp.where(strict, grams[direction][rows, LEN:], 0.0).astype(bf16)
+                pair.append(jnp.where(own[head], erases[direction], mm(feeding, fed_by)))
+            sides.append(tuple(pair))
+    answers = solve_both(couplings, sides, row, col)
     results = []
-    for k, setup in enumerate(setups):
-        _, _, transposes, rights, factors, crossed_values, scale, total = setup
+    for k, (_, _, transposes, crossed_values, scale, total) in enumerate(stages):
         maps, solved = [], []
         for direction in (0, 1):
             for head in (0, 1):
-                mine = head_mask(head)
+                mine = own[head]
                 answer = answers[2 * k + head][direction]
                 rows = jnp.where(mine, answer * scale, answer).astype(bf16)
                 crossed = jnp.where(mine, 0.0, crossed_values).astype(bf16)
                 maps.append(state_map(transposes[direction], rows, crossed, total, head))
                 solved.append(rows)
-        results.append((maps, solved, rights, factors, scale))
+        results.append((maps, solved))
     return results
 
 
@@ -236,13 +230,14 @@
     own = head_mask(0)
     order = (row - col) * (1 - 2 * backward)
     strict = order > 0
-    units = []
-    for pair, low in zip(pairs, lows):
+    gated = []
+    for low in lows:
         gates = jax.nn.sigmoid(bias + low)
         log_decay = jnp.where(own, -DECAY_TOP * gates, 0.0)
-        rate = pltpu.roll(gates, HALF, 1)
+        gated.append((log_decay, pltpu.roll(gates, HALF, 1), cumulative(log_decay, row, col)))
+    stages = []
+    for pair, (log_decay, rate, cum) in zip(pairs, gated):
         keys = jnp.where(own, pair, 0.0)
-        cum = cumulative(log_decay, row, col)
         total = cum[LEN - 1 : LEN]
         half = 0.5 * total
         scale = jnp.exp(half)
@@ -252,13 +247,16 @@
         right = jnp.exp(jnp.where(backward == 0, two, one))
         er, wr, kr = -unit * left, unit * rate * right, keys * right
         grams = mm_nt(er.astype(bf16), jnp.concatenate([wr, kr], axis=0).astype(bf16))
-        coupling = jnp.where(strict, grams[:, :LEN], 0.0)
-        feeding = jnp.where(strict, grams[:, LEN:], 0.0).astype(bf16)
-        crossed = jnp.where(own, 0.0, pair).astype(bf16)
-        side = jnp.where(own, er, mm(feeding, crossed))
         transposed = jnp.concatenate(
             [jnp.transpose(wr * scale), jnp.transpose(kr * scale)], axis=1
         ).astype(bf16)
+        crossed = jnp.where(own, 0.0, pair).astype(bf16)
+        stages.append((grams, er, transposed, crossed, scale, total))
+    units = []
+    for grams, er, transposed, crossed, scale, total in stages:
+        coupling = jnp.where(strict, grams[:, :LEN], 0.0)
+        feeding = jnp.where(strict, grams[:, LEN:], 0.0).astype(bf16)
+        side = jnp.where(own, er, mm(feeding, crossed))
         units.append((coupling, side, transposed, crossed, scale, total))
     answers = solve([u[0] for u in units], [u[1] for u in units], cross)
     maps = []
@@ -346,6 +344,7 @@
     map_out,
     map_in,
     ctx_maps,
+    ctx_state,
     solved_buf,
     right_buf,
     factor_buf,
@@ -612,7 +611,7 @@
         return slot, jnp.where(to == sp, sibling, tp)
 
     def chunk():
-        inputs, at = [], []
+        inputs = []
         for k in range(width // LEN):
             p = k
             cols = slice(p * LEN, (p + 1) * LEN)
@@ -626,25 +625,33 @@
                     rate,
                 )
             )
-            at.append(p)
-        found = pairs_terms(inputs)
-        for p, (maps, solved, rights, factors, scale) in zip(at, found):
+
+        def keep(p, rights, factors, scale):
+            for direction in (0, 1):
+                right_buf[p, direction] = rights[direction]
+                factor_buf[p, direction] = factors[direction]
+            scale_buf[p] = scale
+
+        found = pairs_terms(inputs, keep)
+        for p, (maps, solved) in enumerate(found):
             for direction in (0, 1):
                 for head in (0, 1):
                     map_out[direction * 8 + 2 * p + head] = maps[2 * direction + head].astype(bf16)
         for dz, dy in FAR_FIRST:
             to = at_offset(dz, dy)
             start(remote(map_out.at[to], map_in.at[sp], m_s.at[to], m_r.at[sp], to, tp))
-        for p, (maps, solved, rights, factors, scale) in zip(at, found):
-            for direction in (0, 1):
-                for head in (0, 1):
-                    solved_buf[p, 2 * direction + head] = solved[2 * direction + head]
-                right_buf[p, direction] = rights[direction]
-                factor_buf[p, direction] = factors[direction]
-            scale_buf[p] = scale
+        for p, (maps, solved) in enumerate(found):
+            for i in range(4):
+                solved_buf[p, i] = solved[i]
 
     chunk()
     map_in[sp] = map_out[sp]
+
+    phase("proj_qb")
+    copies[15].wait()
+    project(wq, qbuf, LEN)
+    copies[16].wait()
+    project(wb, bbuf, LEN)
 
     for j in (1, 2, 3):
         frm = (zz + j) % 4
@@ -667,9 +674,27 @@
         lows_in.append(ctx_in[c * per : (c + 1) * per, :, LEN:].astype(f32).reshape(LEN, LEN))
     for c, found in enumerate(context_terms(pairs, lows_in, my_bias, backward)):
         ctx_maps[c] = found
-    phase("proj_b")
-    copies[16].wait()
-    project(wb, bbuf, LEN)
+    count = N_SP // per
+    forward = backward == 0
+    order = [jnp.where(forward, i, N_SP - 1 - i) for i in range(N_SP)]
+    state = ctx_maps[jnp.where(forward, 0, count - 1)]
+    for c in range(1, count):
+        state = compose(state, ctx_maps[jnp.where(forward, c, count - 1 - c)])
+    left = lax.broadcasted_iota(jnp.int32, (1, LEN), 1) < HALF
+
+    def show(i, state):
+        state_out[order[i]] = jnp.where(
+            left, pltpu.roll(state[: HALF // 2], HALF, 1), state[HALF // 2 :]
+        ).astype(bf16)
+
+    def launch(to):
+        slot, over = place(to)
+        remote(state_out.at[to], states.at[slot], s_s.at[to], s_r.at[slot], to, over).start()
+
+    show(0, state)
+    launch(order[0])
+    ctx_state[...] = state
+
     phase("wait_maps")
     for copy in sends:
         copy.wait_send()
@@ -678,56 +703,24 @@
         frm = (sp + j) % N_SP
         remote(map_out.at[0], map_in.at[frm], m_s.at[0], m_r.at[frm], sp, tp).wait_recv()
     phase("walk")
-    count = N_SP // per
-    forward = backward == 0
-    order = [jnp.where(forward, i, N_SP - 1 - i) for i in range(N_SP)]
-    steps = [map_in[order[i]].astype(f32) for i in range(N_SP - 1)]
-    state = ctx_maps[jnp.where(forward, 0, count - 1)]
-    for c in range(1, count):
-        state = compose(state, ctx_maps[jnp.where(forward, c, count - 1 - c)])
-    two = [compose(steps[2 * i], steps[2 * i + 1]) for i in range(7)]
-    four = [compose(two[2 * i], two[2 * i + 1]) for i in range(3)]
-    eight = compose(four[0], four[1])
-    odd = my_head % 2
-    left = lax.broadcasted_iota(jnp.int32, (1, LEN), 1) < HALF
-
-    def show(i, state):
-        to = order[i]
-        state_out[to] = jnp.where(
-            left, pltpu.roll(state[: HALF // 2], HALF, 1), state[HALF // 2 :]
-        ).astype(bf16)
-
-    def launch(to):
-        slot, over = place(to)
-        remote(state_out.at[to], states.at[slot], s_s.at[to], s_r.at[slot], to, over).start()
-
-    held = {0: state}
-    show(0, state)
-    held[8] = compose(state, eight)
-    held[4] = compose(state, four[0])
-    show(8, held[8])
-    show(4, held[4])
-    for i in (0, 8, 4):
-        launch(order[i])
-    held[12] = compose(held[8], four[2])
-    held[2] = compose(state, two[0])
-    held[6] = compose(held[4], two[2])
-    held[10] = compose(held[8], two[4])
-    held[14] = compose(held[12], two[6])
-    for i in (2, 6, 10, 12, 14):
-        show(i, held[i])
-    for i in (2, 6, 10, 12, 14):
-        launch(order[i])
-    for i in range(1, N_SP, 2):
-        show(i, compose(held[i - 1], steps[i - 1]))
-    even = (yy % 2 == 0) == (backward == 1)
-    for one, other in zip(EVEN_FIRST, ODD_FIRST):
-        launch(jnp.where(even, at_offset(*one), at_offset(*other)))
+    held = [ctx_state[...]] + [map_in[order[i]].astype(f32) for i in range(N_SP - 1)]
+    size = 1
+    while size < N_SP:
+        held = [
+            compose(held[i // size * size - 1], h) if i & size else h for i, h in enumerate(held)
+        ]
+        for i in range(size, 2 * size):
+            show(i, held[i])
+        if size < N_SP // 2:
+            for i in range(size, 2 * size):
+                launch(order[i])
+        size *= 2
+    base = jnp.where(forward, 2, 0)
+    for dy in (2, 1, 3, 0):
+        for k in (0, 1):
+            launch((base + (zz + k) % 2) * 4 + (yy + dy) % 4)
     states[sp] = state_out[sp]
 
-    phase("proj_qb")
-    copies[15].wait()
-    project(wq, qbuf, LEN)
     phase("read_terms")
 
     def read_terms(p, carry):
@@ -954,6 +947,7 @@
         V((N_SP, HALF, LEN), bf16),
         V((N_SP + 1, HALF, LEN), bf16),
         V((4, HALF, LEN), f32),
+        V((HALF, LEN), f32),
         V((width // LEN, 4, LEN, LEN), bf16),
         V((width // LEN, 2, 2 * LEN, LEN), bf16),
         V((width // LEN, 2, LEN, LEN), f32),

time: 51.6 us -> 49.8 us (0.965)
  Pallas kernels: 50.8 us -> 49 us
    pallas_call x1, Pallas kernels: 50.8 us -> 49 us  [on_device(): pl.pallas_call(kernel, out_shape=jax.ShapeDtypeStruct((own_n, model), bf1...]
where the time goes in v5:
time: 49.8 us; the launch traced here: 49.7 us
  Pallas kernels  49 us (98%)
  local copies, waits for them, and re-layouts  0.66 us (1%)
    pallas_call x1, Pallas kernels, on_device(): pl.pallas_call(kernel, out_shape=jax.ShapeDtypeStruct((own_n, model), bf1...  49 us

profile of v5, /device:TPU:1, one launch (start us, length us, event | category | flops | bytes accessed | tf_op | source)
XLA Modules:
  0.0 49.7 jit_solution(13223522716928890080)
XLA Ops:
  0.0 49.0 %shard_map.181 = bf16[16,4096]{1,0:T(8,128)(2,1)S(1)} custom-call(bf16[16,4096]{1,0:T(8,128)(2,1)} %latent.1, bf16[32,4096]{1,0:T(8,128)(2,1)} %context.1, f32[1,256]{1,0:T(1,128)} %bitcast.6, f32[1,256]{1,0:T(1,128)} %bitcast.7, bf16[256,512]{1,0:T(8,128)(2,1)} %shift_weight.1, bf16[256,512]{1,0:T(8,128)(2,1)} %scale_weight.1, ...), custom_call_target="tpu_custom_call" | custom-call | tf_op jit(solution)/shard_map/pallas_call | solution.py:989
  49.1 0.7 %copy.21 = bf16[16,4096]{1,0:T(8,128)(2,1)} copy(bf16[16,4096]{1,0:T(8,128)(2,1)S(1)} %shard_map.181) | data formatting | bytes 262144
